TPU v7x, 256 devices: a whole 4x4x8 slice. The times are simulated.
256 devices in a mesh: sp: 64 (over z, y, core), tp: 4 (over x).
Axes of the slice: x: 4, y: 4, z: 8, core: 2. Of those that a mesh axis runs over, the one named last changes fastest.
Arguments:
- grad_out: bfloat16 [16384, 2048], P('sp'), may hold values from -16 to 16
- resid: bfloat16 [16384, 2048], P('sp'), may hold values from -6 to 6
- norm_gain: float32 [2048], replicated, may hold values from 0.1 to 1.9
- routes: int32 [16384, 2], P('sp'), may hold values from 0 to 63, all different within a row; in each aligned block of 256 rows (0 to 255, 256 to 511, ...) at most 12 rows name the same one
- route_weights: float32 [16384, 2], P('sp'), may hold values from 0.05 to 1
- gate_weight: bfloat16 [64, 2048, 1536], P('sp', None, 'tp'), may hold values from -0.375 to 0.375
- up_weight: bfloat16 [64, 2048, 1536], P('sp', None, 'tp'), may hold values from -0.375 to 0.375
- down_weight: bfloat16 [64, 1536, 2048], P('sp', 'tp'), may hold values from -0.15625 to 0.15625
- proj_weight: bfloat16 [2048, 512], P(None, 'tp'), may hold values from -0.25 to 0.25
- conv_sum: bfloat16 [16384, 512], P('sp', 'tp'), may hold values from -6 to 6
- conv_gain: float32 [512], P('tp'), may hold values from 0.1 to 1.9
- conv_taps: float32 [31, 512], P(None, 'tp'), may hold values from -1 to 1
- conv_value: bfloat16 [16384, 512], P('sp', 'tp'), may hold values from -6 to 6
- conv_gate: bfloat16 [16384, 512], P('sp', 'tp'), may hold values from -6 to 6
Outputs:
- gate_weight_grad: bfloat16 [64, 2048, 1536], P('sp', None, 'tp')
- up_weight_grad: bfloat16 [64, 2048, 1536], P('sp', None, 'tp')
- down_weight_grad: bfloat16 [64, 1536, 2048], P('sp', 'tp')
- proj_grad: float32 [2048, 512], P('sp', 'tp')
- value_grad: bfloat16 [16384, 512], P('sp', 'tp')
- gate_input_grad: bfloat16 [16384, 512], P('sp', 'tp')
Inputs may be any that keep to these rules, and one draw needn't show every extreme that they name: In each aligned block of 256 tokens no expert is named by more than 12 routes, and in some block one expert is named exactly 12 times; a token's two routes name different experts.
All inputs are finite; a program needn't handle non-finite values.
Results may differ from a plain program's by a relative error of at most 0.028.
Values may be sent and summed in bfloat16 or wider, within the bound.
A program may use at most 128 MiB of HBM per device.

v0:
```python
import jax
import jax.numpy as jnp
from jax import lax
from jax.sharding import PartitionSpec as P

CONV_K = 31
GROUP = 128


CLAMP_LIMIT = 7.0
SLOPE_ALPHA = 1.702


def sent_to_all(shard, axis):
    peers = lax.axis_size(axis)
    return lax.all_to_all(
        jnp.broadcast_to(shard[None], (peers, *shard.shape)), axis, 0, 0, tiled=True
    )


def laid_out(parts, dim):
    parts = jnp.moveaxis(parts, 0, dim)
    shape = parts.shape
    return parts.reshape(*shape[:dim], shape[dim] * shape[dim + 1], *shape[dim + 2 :])


def collect(shard, axis, dim):
    parts = sent_to_all(shard, axis)
    return laid_out(parts, dim)


def split_up(shard, dim, peers):
    shape = shard.shape
    parts = shard.reshape(*shape[:dim], peers, shape[dim] // peers, *shape[dim + 1 :])
    return jnp.moveaxis(parts, dim, 0)


def summed_on_arrival(shard, axis, dim):
    parts = split_up(shard, dim, lax.axis_size(axis))
    arrived = lax.all_to_all(parts, axis, split_axis=0, concat_axis=0, tiled=True)
    return arrived.astype(jnp.float32).sum(axis=0)


def passed_along(block, axis, distance):
    devices = range(lax.axis_size(axis))
    route = [(i - distance, i) for i in devices if i - distance in devices]
    return lax.ppermute(block, axis, route)


def contract_rows(left_side, right_side):
    return lax.dot_general(
        left_side, right_side, (((0,), (0,)), ((), ())), preferred_element_type=jnp.float32
    )


def contract_cols(left_side, right_side):
    return lax.dot_general(
        left_side, right_side, (((1,), (1,)), ((), ())), preferred_element_type=jnp.float32
    )


def expert_backward(routed_rows, routed_cots, w_gate, w_up, w_down):
    gate_pre = jnp.dot(routed_rows, w_gate, preferred_element_type=jnp.float32)
    up_pre = jnp.dot(routed_rows, w_up, preferred_element_type=jnp.float32)
    gate_clamped = jnp.minimum(gate_pre, CLAMP_LIMIT)
    up_clamped = jnp.clip(up_pre, -CLAMP_LIMIT, CLAMP_LIMIT)
    sigma = jax.nn.sigmoid(SLOPE_ALPHA * gate_clamped)
    gated = gate_clamped * sigma
    act = ((up_clamped + 1.0) * gated).astype(jnp.bfloat16)
    down_grad = contract_rows(act, routed_cots).astype(jnp.bfloat16)
    act_grad = contract_cols(routed_cots, w_down)
    inside = (up_pre > -CLAMP_LIMIT) & (up_pre < CLAMP_LIMIT)
    up_pre_grad = jnp.where(inside, act_grad * gated, 0.0).astype(jnp.bfloat16)
    slope = sigma + SLOPE_ALPHA * gate_clamped * sigma * (1.0 - sigma)
    gate_pre_grad = jnp.where(
        gate_pre < CLAMP_LIMIT, act_grad * (up_clamped + 1.0) * slope, 0.0
    ).astype(jnp.bfloat16)
    gate_grad = contract_rows(routed_rows, gate_pre_grad).astype(jnp.bfloat16)
    up_grad = contract_rows(routed_rows, up_pre_grad).astype(jnp.bfloat16)
    partial_value = contract_cols(gate_pre_grad, w_gate) + contract_cols(up_pre_grad, w_up)
    return (gate_grad, up_grad, down_grad, partial_value)


def local(
    grad_out,
    resid,
    norm_gain,
    routes,
    route_weights,
    gate_weight,
    up_weight,
    down_weight,
    proj_weight,
    conv_sum,
    conv_gain,
    conv_taps,
    conv_value,
    conv_gate,
):
    tok_rows, model_width = resid.shape
    sp_count = lax.axis_size("sp")
    tp_count = lax.axis_size("tp")
    capacity = 3 * tok_rows // sp_count
    col_count = model_width // tp_count
    resid_f = resid.astype(jnp.float32)
    inv_rms = lax.rsqrt(jnp.mean(resid_f * resid_f, axis=-1, keepdims=True) + 1e-06)
    normed = (resid_f * inv_rms * norm_gain).astype(jnp.bfloat16)
    scaled = (route_weights[:, :, None] * grad_out.astype(jnp.float32)[:, None, :]).astype(
        jnp.bfloat16
    )
    scaled = scaled.reshape(2 * tok_rows, model_width)
    route_ids = routes.reshape(-1)
    one_hot = (route_ids[:, None] == jnp.arange(sp_count, dtype=jnp.int32)[None, :]).astype(
        jnp.int32
    )
    slot_rank = jnp.sum(jnp.cumsum(one_hot, axis=0) * one_hot, axis=1) - 1
    slot_index = route_ids * capacity + slot_rank
    slot_table = jnp.full((sp_count * capacity,), 2 * tok_rows, jnp.int32)
    slot_table = slot_table.at[slot_index].set(jnp.arange(2 * tok_rows, dtype=jnp.int32))
    normed_pad = jnp.concatenate([normed, jnp.zeros((1, model_width), jnp.bfloat16)], axis=0)
    scaled_pad = jnp.concatenate([scaled, jnp.zeros((1, model_width), jnp.bfloat16)], axis=0)
    first_col = lax.axis_index("tp") * col_count
    normed_part = lax.dynamic_slice_in_dim(normed_pad, first_col, col_count, 1)
    scaled_part = lax.dynamic_slice_in_dim(scaled_pad, first_col, col_count, 1)
    send_rows = normed_part[slot_table // 2].reshape(sp_count, capacity, col_count)
    send_cots = scaled_part[slot_table].reshape(sp_count, capacity, col_count)
    part_rows, part_cots = (
        lax.all_to_all(send_rows, "sp", split_axis=0, concat_axis=0, tiled=True),
        lax.all_to_all(send_cots, "sp", split_axis=0, concat_axis=0, tiled=True),
    )
    routed_rows, routed_cots = (
        lax.all_gather(part_rows, "tp", axis=2, tiled=True),
        lax.all_gather(part_cots, "tp", axis=2, tiled=True),
    )
    routed_rows = routed_rows.reshape(sp_count * capacity, model_width)
    routed_cots = routed_cots.reshape(sp_count * capacity, model_width)
    gate_grad, up_grad, down_grad, partial_value = expert_backward(
        routed_rows, routed_cots, gate_weight[0], up_weight[0], down_weight[0]
    )
    row_grad = lax.psum_scatter(
        partial_value.reshape(sp_count, capacity, model_width).astype(jnp.bfloat16),
        "tp",
        scatter_dimension=2,
        tiled=True,
    )
    returned = lax.all_to_all(row_grad, "sp", split_axis=0, concat_axis=0, tiled=True).reshape(
        sp_count * capacity, col_count
    )
    normed_part_grad = returned[slot_index].reshape(tok_rows, 2, col_count).astype(jnp.float32)
    normed_part_grad = normed_part_grad.sum(axis=1).astype(jnp.bfloat16)
    normed_grad = collect(normed_part_grad, "tp", 1)
    feature_grad = normed_grad.astype(jnp.float32) * norm_gain
    cubed = inv_rms * inv_rms * inv_rms
    resid_grad = (
        grad_out.astype(jnp.float32)
        + inv_rms * feature_grad
        - resid_f * cubed * jnp.mean(resid_f * feature_grad, axis=-1, keepdims=True)
    ).astype(jnp.bfloat16)
    channels = conv_sum.shape[1]
    summed = conv_sum.astype(jnp.float32).reshape(tok_rows, channels // GROUP, GROUP)
    centre = summed - jnp.mean(summed, axis=-1, keepdims=True)
    inv_std = lax.rsqrt(jnp.mean(centre * centre, axis=-1, keepdims=True) + 1e-05)
    grouped = centre * inv_std
    chan_normed = grouped.reshape(tok_rows, channels)
    pre_act = chan_normed * conv_gain
    sigma_conv = jax.nn.sigmoid(pre_act)
    conv_out = (pre_act * sigma_conv).astype(jnp.bfloat16)
    proj_grad = summed_on_arrival(contract_rows(resid_grad, conv_out).astype(jnp.bfloat16), "sp", 0)
    out_grad = jnp.dot(resid_grad, proj_weight, preferred_element_type=jnp.float32)
    normal_grad = (
        out_grad * sigma_conv * (1.0 + pre_act * (1.0 - sigma_conv)) * conv_gain
    ).reshape(tok_rows, channels // GROUP, GROUP)
    sum_grad = inv_std * (
        normal_grad
        - jnp.mean(normal_grad, axis=-1, keepdims=True)
        - grouped * jnp.mean(normal_grad * grouped, axis=-1, keepdims=True)
    )
    sum_grad = sum_grad.reshape(tok_rows, channels)
    following = passed_along(sum_grad[: CONV_K - 1], "sp", -1)
    extended = jnp.concatenate([sum_grad, following], axis=0)
    gated_grad = lax.conv_general_dilated(
        extended[None],
        conv_taps[::-1][:, None, :],
        (1,),
        ((0, 0),),
        dimension_numbers=("NWC", "WIO", "NWC"),
        feature_group_count=channels,
        precision=lax.Precision.HIGHEST,
    )[0]
    sigma_gate = jax.nn.sigmoid(conv_gate.astype(jnp.float32))
    value_grad = (gated_grad * sigma_gate).astype(jnp.bfloat16)
    gate_input_grad = (
        gated_grad * conv_value.astype(jnp.float32) * sigma_gate * (1.0 - sigma_gate)
    ).astype(jnp.bfloat16)
    return (gate_grad[None], up_grad[None], down_grad[None], proj_grad, value_grad, gate_input_grad)


def solution(mesh):
    in_specs = (
        P("sp", None),
        P("sp", None),
        P(),
        P("sp", None),
        P("sp", None),
        P("sp", None, "tp"),
        P("sp", None, "tp"),
        P("sp", "tp", None),
        P(None, "tp"),
        P("sp", "tp"),
        P("tp"),
        P(None, "tp"),
        P("sp", "tp"),
        P("sp", "tp"),
    )
    out_specs = (
        P("sp", None, "tp"),
        P("sp", None, "tp"),
        P("sp", "tp", None),
        P("sp", "tp"),
        P("sp", "tp"),
        P("sp", "tp"),
    )
    return jax.shard_map(local, mesh=mesh, in_specs=in_specs, out_specs=out_specs, check_vma=False)
```

profile of v0, /device:TPU:1, one launch (start us, length us, event | category | flops | bytes accessed | tf_op | source)
XLA Modules:
  0.0 337.3 jit_solution(5426419084844217634)
XLA Ops:
  7.3 0.8 broadcast_multiply_fusion
  8.1 0.8 copy.34
  8.9 0.1 eq.25
  9.1 0.1 eq.29
  9.2 1.5 fusion.3
  10.7 0.1 copy.33
  10.9 0.1 mul.210
  11.0 1.2 reduce-window.6
  12.2 0.2 slice_reduce_fusion
  12.5 0.1 fusion.48
  12.7 2.4 scatter_custom_fusion
  15.2 0.3 fusion.5
  15.5 3.3 gather_fusion
  18.9 2.1 reshape.174
  20.9 41.4 %all_to_all.25 = bf16[64,12,512]{2,1,0:T(8,128)(2,1)} all-to-all(bf16[64,12,512]{2,1,0:T(8,128)(2,1)} %reshape.174), channel_id=1, replica_groups=mesh['sp'=64,'tp'=4] {'sp'}, dimensions={0} | all-to-all | bytes 1572864 | tf_op jit(solution)/shard_map/all_to_all | solution.py:128
  62.4 5.3 %mul.214 = f32[256,2,2048]{2,1,0:T(2,128)} broadcast(bf16[256,2048]{1,0:T(8,128)(2,1)} %param.14), dimensions={0,2} | broadcast | bytes 5242880 | tf_op jit(solution)/shard_map/mul | solution.py:108
  67.8 6.2 %mul.215 = f32[512,2048]{1,0:T(8,128)} reshape(f32[256,2,2048]{2,1,0:T(2,128)} %mul.214) | data formatting | bytes 8388608 | tf_op jit(solution)/shard_map/mul | solution.py:108
  74.0 0.1 copy.37
  74.1 0.1 mul.212
  74.3 2.5 multiply_convert_fusion
  76.9 3.3 gather_fusion.1
  80.2 2.1 reshape.176
  82.3 34.7 %all_to_all.26 = bf16[64,12,512]{2,1,0:T(8,128)(2,1)} all-to-all(bf16[64,12,512]{2,1,0:T(8,128)(2,1)} %reshape.176), channel_id=1, replica_groups=mesh['sp'=64,'tp'=4] {'sp'}, dimensions={0} | all-to-all | bytes 1572864 | tf_op jit(solution)/shard_map/all_to_all | solution.py:129
  117.0 0.2 reduce-scatter.2.cloned.1.call-start
  117.3 6.2 %reshape.175 = bf16[768,2048]{1,0:T(8,128)(2,1)} reshape(bf16[64,12,2048]{2,1,0:T(8,128)(2,1)} %all-gather.3.cloned.1.call-done) | data formatting | bytes 6291456 | tf_op jit(solution)/shard_map/reshape | solution.py:135
  123.5 5.5 %fusion.11 = f32[768,384]{1,0:T(8,128)} fusion(bf16[768,2048]{1,0:T(8,128)(2,1)} %reshape.175, bf16[1,2048,384]{2,1,0:T(8,128)(2,1)} %param.20), kind=kOutput, calls=%fused_computation.27 | convolution fusion | flops 1207959552 | bytes 5898240 | tf_op jit(solution)/shard_map/dot_general | solution.py:64
  129.0 2.8 fusion.17
  131.8 32.9 %all-gather.5.cloned.1.call-done = bf16[64,12,2048]{2,1,0:T(8,128)(2,1)} async-done(((bf16[64,12,512]{2,1,0:T(8,128)(2,1)}), bf16[64,12,2048]{2,1,0:T(8,128)(2,1)}) %all-gather.5.cloned.1.call-update) | async-done | bytes 3145744 | tf_op jit(solution)/shard_map/all_gather | solution.py:133
  164.7 6.1 %reshape.177 = bf16[768,2048]{1,0:T(8,128)(2,1)} reshape(bf16[64,12,2048]{2,1,0:T(8,128)(2,1)} %all-gather.5.cloned.1.call-done) | data formatting | bytes 6291456 | tf_op jit(solution)/shard_map/reshape | solution.py:136
  170.8 5.5 %select_convert_fusion = (bf16[768,384]{1,0:T(8,128)(2,1)S(1)}, bf16[768,384]{1,0:T(8,128)(2,1)S(1)}) fusion(f32[768,384]{1,0:T(8,128)} %fusion.11, f32[768,384]{1,0:T(8,128)} %fusion.17, bf16[768,2048]{1,0:T(8,128)(2,1)} %reshape.177, bf16[1,384,2048]{2,1,0:T(8,128)(2,1)} %param.21), kind=kOutput, calls=%fused_computation.36 | convolution fusion | flops 1214742528 | bytes 8257536 | tf_op jit(solution)/shard_map/dot_general | solution.py:57
  176.3 1.8 fusion.15
  178.2 3.5 %add_convert_fusion = bf16[768,2048]{1,0:T(8,128)(2,1)} fusion(f32[768,2048]{1,0:T(8,128)S(1)} %fusion.15, bf16[768,384]{1,0:T(8,128)(2,1)S(1)} %get-tuple-element.8, bf16[1,2048,384]{2,1,0:T(8,128)(2,1)S(1)} %copy-done.6), kind=kOutput, calls=%fused_computation.4 | convolution fusion | flops 1211105280 | bytes 11599872 | tf_op jit(solution)/shard_map/dot_general | solution.py:57
  181.7 6.1 %convert_element_type.93 = bf16[64,12,2048]{2,1,0:T(8,128)(2,1)} reshape(bf16[768,2048]{1,0:T(8,128)(2,1)} %add_convert_fusion) | data formatting | bytes 6291456 | tf_op jit(solution)/shard_map/convert_element_type | solution.py:141
  187.8 50.0 %reduce-scatter.2.cloned.1.call-done = bf16[64,12,512]{2,1,0:T(8,128)(2,1)} async-done(((bf16[64,12,2048]{2,1,0:T(8,128)(2,1)}), bf16[64,12,512]{2,1,0:T(8,128)(2,1)}) %reduce-scatter.2.cloned.1.call-update) | async-done | bytes 786448 | tf_op jit(solution)/shard_map/reduce_scatter | solution.py:140
  237.8 11.0 %all-to-all-start.2 = ((bf16[64,12,512]{2,1,0:T(8,128)(2,1)}), bf16[64,12,512]{2,1,0:T(8,128)(2,1)}, u32[]{:S(2)}, u32[]{:S(2)}) async-start(bf16[64,12,512]{2,1,0:T(8,128)(2,1)} %reduce-scatter.2.cloned.1.call-done), calls=%async_computation.3 | async-start | bytes 2097152 | tf_op jit(solution)/shard_map/all_to_all | solution.py:146
  248.8 0.1 convert_reduce_fusion.1
  248.9 0.2 fusion.46
  249.1 27.7 %all-to-all-done.2 = bf16[64,12,512]{2,1,0:T(8,128)(2,1)} async-done(((bf16[64,12,512]{2,1,0:T(8,128)(2,1)}), bf16[64,12,512]{2,1,0:T(8,128)(2,1)}, u32[]{:S(2)}, u32[]{:S(2)}) %all-to-all-start.2) | async-done | bytes 786464 | tf_op jit(solution)/shard_map/all_to_all | solution.py:146
  276.8 1.3 reshape.178
  278.1 2.0 gather_fusion.2
  280.1 0.2 reshape.179
  280.3 1.4 reduce_sum.86
  281.7 1.1 broadcast_in_dim.57
  282.8 3.7 %all-to-all-start.3 = ((bf16[4,256,512]{2,1,0:T(8,128)(2,1)}), bf16[4,256,512]{2,1,0:T(8,128)(2,1)S(1)}, u32[]{:S(2)}, u32[]{:S(2)}) async-start(bf16[4,256,512]{2,1,0:T(8,128)(2,1)} %broadcast_in_dim.57), calls=%async_computation.4 | async-start | bytes 2097152 | tf_op jit(solution)/shard_map/all_to_all | solution.py:16
  286.5 5.0 %fusion = bf16[1,2048,384]{2,1,0:T(8,128)(2,1)} fusion(bf16[768,2048]{1,0:T(8,128)(2,1)} %reshape.175, bf16[768,384]{1,0:T(8,128)(2,1)S(1)} %get-tuple-element.9), kind=kOutput, calls=%fused_computation.13 | convolution fusion | flops 1208745984 | bytes 5308416 | tf_op jit(solution)/shard_map/dot_general | solution.py:51
  291.6 2.7 fusion.2
  294.3 6.0 %all-to-all-done.3 = bf16[4,256,512]{2,1,0:T(8,128)(2,1)S(1)} async-done(((bf16[4,256,512]{2,1,0:T(8,128)(2,1)}), bf16[4,256,512]{2,1,0:T(8,128)(2,1)S(1)}, u32[]{:S(2)}, u32[]{:S(2)}) %all-to-all-start.3) | async-done | bytes 1048608 | tf_op jit(solution)/shard_map/all_to_all | solution.py:16
  300.3 0.3 convert_bitcast_fusion
  300.6 0.2 copy.44
  300.8 0.4 fusion.9
  301.2 0.8 copy-done.3
  302.0 0.7 fusion.8
  302.7 1.0 copy-done.7
  303.6 1.4 convolution_convert_fusion.3
  305.0 7.4 %all-to-all-start.4 = ((bf16[64,32,128]{2,1,0:T(8,128)(2,1)}), bf16[64,32,128]{2,1,0:T(8,128)(2,1)S(1)}, u32[]{:S(2)}, u32[]{:S(2)}) async-start(bf16[64,32,128]{2,1,0:T(8,128)(2,1)} %bitcast.10), calls=%async_computation.5 | async-start | bytes 1048576 | tf_op jit(solution)/shard_map/all_to_all | solution.py:40
  312.4 1.8 fusion.67
  314.3 0.2 fusion.45
  314.5 2.4 collective-permute-start
  316.9 4.9 %fusion.1 = bf16[1,2048,384]{2,1,0:T(8,128)(2,1)} fusion(bf16[768,2048]{1,0:T(8,128)(2,1)} %reshape.175, bf16[768,384]{1,0:T(8,128)(2,1)S(1)} %copy-done.9), kind=kOutput, calls=%fused_computation.14 | convolution fusion | flops 1208745984 | bytes 5308416 | tf_op jit(solution)/shard_map/dot_general | solution.py:51
  321.9 0.3 convolution_select_fusion
  322.3 0.5 copy-done.12
  322.8 0.7 multiply_convert_fusion.3
  323.6 6.5 %all-to-all-done.4 = bf16[64,32,128]{2,1,0:T(8,128)(2,1)S(1)} async-done(((bf16[64,32,128]{2,1,0:T(8,128)(2,1)}), bf16[64,32,128]{2,1,0:T(8,128)(2,1)S(1)}, u32[]{:S(2)}, u32[]{:S(2)}) %all-to-all-start.4) | async-done | bytes 524320 | tf_op jit(solution)/shard_map/all_to_all | solution.py:40
  330.1 0.7 convert_reduce_fusion
  (71 shorter events, 0.6 us)
Async XLA Ops:
  7.2 121.8 %copy-start = (bf16[1,2048,384]{2,1,0:T(8,128)(2,1)S(1)}, bf16[1,2048,384]{2,1,0:T(8,128)(2,1)}, u32[]{:S(2)}) copy-start(bf16[1,2048,384]{2,1,0:T(8,128)(2,1)} %param.19) | copy-start | bytes 4718596
  7.2 8.0 %copy-start.2 = (bf16[256,2048]{1,0:T(8,128)(2,1)S(1)}, bf16[256,2048]{1,0:T(8,128)(2,1)}, u32[]{:S(2)}) copy-start(bf16[256,2048]{1,0:T(8,128)(2,1)} %param.15) | copy-start | bytes 3145732
  7.2 8.0 %copy-start.11 = (f32[2048]{0:T(1024)S(1)}, f32[2048]{0:T(1024)}, u32[]{:S(2)}) copy-start(f32[2048]{0:T(1024)} %param.16) | copy-start | bytes 24580
  7.2 110.1 %all-gather.3.cloned.1.call-start = ((), (), s32[]{:S(2)}) async-start(), calls=%async_computation.6 | async-start | bytes 5242880 | tf_op jit(solution)/shard_map/all_gather | solution.py:132
  62.4 102.3 %all-gather.5.cloned.1.call-start = ((), (), s32[]{:S(2)}) async-start(), calls=%async_computation.7 | async-start | bytes 5242880 | tf_op jit(solution)/shard_map/all_gather | solution.py:133
  67.8 6.2 %copy-start.15 = (f32[256,2]{0,1:T(2,128)S(1)}, f32[256,2]{0,1:T(2,128)}, u32[]{:S(2)}) copy-start(f32[256,2]{0,1:T(2,128)} %param.18) | copy-start | bytes 6148
  117.0 120.7 %reduce-scatter.2.cloned.1.call-start = ((), (), s32[]{:S(2)}) async-start(), calls=%async_computation.8 | async-start | bytes 5242880 | tf_op jit(solution)/shard_map/reduce_scatter | solution.py:140
  123.5 5.5 %copy-start.4 = (bf16[768,2048]{1,0:T(8,128)(2,1)S(1)}, bf16[768,2048]{1,0:T(8,128)(2,1)}, u32[]{:S(2)}) copy-start(bf16[768,2048]{1,0:T(8,128)(2,1)} %reshape.175) | copy-start | bytes 9437188
  176.3 1.9 copy-start.8
  176.3 1.9 copy-start.6
  187.8 61.0 %copy-start.14 = (f32[31,128]{1,0:T(8,128)S(1)}, f32[31,128]{1,0:T(8,128)}, u32[]{:S(2)}) copy-start(f32[31,128]{1,0:T(8,128)} %param.25) | copy-start | bytes 47620
  187.8 61.0 %copy-start.10 = (bf16[256,128]{1,0:T(8,128)(2,1)S(1)}, bf16[256,128]{1,0:T(8,128)(2,1)}, u32[]{:S(2)}) copy-start(bf16[256,128]{1,0:T(8,128)(2,1)} %param.23) | copy-start | bytes 196612
  237.8 39.0 %all-to-all-start.2 = ((bf16[64,12,512]{2,1,0:T(8,128)(2,1)}), bf16[64,12,512]{2,1,0:T(8,128)(2,1)}, u32[]{:S(2)}, u32[]{:S(2)}) async-start(bf16[64,12,512]{2,1,0:T(8,128)(2,1)} %reduce-scatter.2.cloned.1.call-done), calls=%async_computation.3 | async-start | bytes 2097152 | tf_op jit(solution)/shard_map/all_to_all | solution.py:146
  282.8 17.5 %all-to-all-start.3 = ((bf16[4,256,512]{2,1,0:T(8,128)(2,1)}), bf16[4,256,512]{2,1,0:T(8,128)(2,1)S(1)}, u32[]{:S(2)}, u32[]{:S(2)}) async-start(bf16[4,256,512]{2,1,0:T(8,128)(2,1)} %broadcast_in_dim.57), calls=%async_computation.4 | async-start | bytes 2097152 | tf_op jit(solution)/shard_map/all_to_all | solution.py:16
  286.5 5.1 %copy-start.5 = (bf16[768,2048]{1,0:T(8,128)(2,1)S(1)}, bf16[768,2048]{1,0:T(8,128)(2,1)}, u32[]{:S(2)}) copy-start(bf16[768,2048]{1,0:T(8,128)(2,1)} %reshape.177) | copy-start | bytes 9437188
  286.5 5.1 %copy-start.19 = (f32[768,384]{1,0:T(8,128)S(1)}, f32[768,384]{1,0:T(8,128)}, u32[]{:S(2)}) copy-start(f32[768,384]{1,0:T(8,128)} %fusion.11) | copy-start | bytes 3538948
  286.5 5.0 %copy-start.20 = (f32[768,384]{1,0:T(8,128)S(1)}, f32[768,384]{1,0:T(8,128)}, u32[]{:S(2)}) copy-start(f32[768,384]{1,0:T(8,128)} %fusion.17) | copy-start | bytes 3538948
  300.8 1.2 copy-start.3
  302.0 1.6 copy-start.17
  302.7 1.0 copy-start.7
  303.6 8.8 %copy-start.16 = (bf16[2048,128]{1,0:T(8,128)(2,1)S(1)}, bf16[2048,128]{1,0:T(8,128)(2,1)}, u32[]{:S(2)}) copy-start(bf16[2048,128]{1,0:T(8,128)(2,1)} %param.22) | copy-start | bytes 1572868
  305.0 25.1 %all-to-all-start.4 = ((bf16[64,32,128]{2,1,0:T(8,128)(2,1)}), bf16[64,32,128]{2,1,0:T(8,128)(2,1)S(1)}, u32[]{:S(2)}, u32[]{:S(2)}) async-start(bf16[64,32,128]{2,1,0:T(8,128)(2,1)} %bitcast.10), calls=%async_computation.5 | async-start | bytes 1048576 | tf_op jit(solution)/shard_map/all_to_all | solution.py:40
  312.4 4.5 %copy-start.9 = (bf16[768,384]{1,0:T(8,128)(2,1)S(1)}, bf16[768,384]{1,0:T(8,128)(2,1)}, u32[]{:S(2)}) copy-start(bf16[768,384]{1,0:T(8,128)(2,1)} %copy-done.8) | copy-start | bytes 1769476
  314.5 7.4 %copy-start.18 = (pred[8,36]{0,1:T(8,128)(4,1)S(1)}, pred[8,36]{0,1:T(8,128)(4,1)}, u32[]{:S(2)}) copy-start(pred[8,36]{0,1:T(8,128)(4,1)} %constant.83) | copy-start | bytes 868
  314.5 7.3 %collective-permute-start = (f32[30,128]{1,0:T(8,128)S(1)}, f32[30,128]{1,0:T(8,128)S(1)}, u32[]{:S(2)}, u32[]{:S(2)}) collective-permute-start(f32[30,128]{1,0:T(8,128)S(1)} %slice.23), channel_id=1, source_target_pairs={{4,0},{8,4},{12,8},{16,12},{20,16},{24,20},{28,24},{32,28},{36,32}... | collective-permute-start | bytes 46088 | tf_op jit(solution)/shard_map/ppermute | solution.py:47
  321.8 9.0 %copy-start.1 = (bf16[1,2048,384]{2,1,0:T(8,128)(2,1)S(1)}, bf16[1,2048,384]{2,1,0:T(8,128)(2,1)}, u32[]{:S(2)}) copy-start(bf16[1,2048,384]{2,1,0:T(8,128)(2,1)} %param.19) | copy-start | bytes 4718596
  321.9 1.0 copy-start.12
  321.9 1.0 copy-start.13
Sparse Core Ops, SparseCore 0:
  62.5 47.4 all-gather.2
  117.2 47.4 all-gather.4
  187.9 49.8 reduce-scatter.1
where the time goes:
time: 339 us; the launch traced here: 337 us
  waiting for transfers between devices  123 us (36%)
  blocking collectives  76.1 us (22%)
  local copies, waits for them, and re-layouts  52.4 us (15%)
  matrix products  35.3 us (10%)
  starting transfers between devices  24.7 us (7%)
  between operations  14.3 us (4%)
  other arithmetic  11.3 us (3%)
    reduce_scatter x1, waiting for transfers between devices, local(): lax.psum_scatter(partial_value.reshape(sp_count, capacity, model_width).a...  50 us
    all_to_all x1, blocking collectives, local(): lax.all_to_all(send_rows, 'sp', split_axis=0, concat_axis=0, tiled=True)  41.4 us
    all_to_all x1, blocking collectives, local(): lax.all_to_all(send_cots, 'sp', split_axis=0, concat_axis=0, tiled=True)  34.7 us
    all_gather x1, waiting for transfers between devices, local(): lax.all_gather(part_cots, 'tp', axis=2, tiled=True)  32.9 us
    all_to_all x1, waiting for transfers between devices, local(): lax.all_to_all(row_grad, 'sp', split_axis=0, concat_axis=0, tiled=True)  27.7 us
    dot_general x4, matrix products, contract_rows(): lax.dot_general(left_side, right_side, (((0,), (0,)), ((), ())), preferre...  14 us
    mul x3, local copies, waits for them, and re-layouts, local(): route_weights[:, :, None] * grad_out.astype(jnp.float32)[:, None, :]  11.7 us
    all_to_all x1, starting transfers between devices, local(): lax.all_to_all(row_grad, 'sp', split_axis=0, concat_axis=0, tiled=True)  11 us
  transfers between devices with their start and end apart: 7, of which 5 were waited for; matrix products, arithmetic and copies ran while one was open for 15% of the time, Pallas kernels for 0%

commit v1 on v0

--- a/solution.py
+++ b/solution.py
@@ -1,14 +1,243 @@
+import functools
+
 import jax
 import jax.numpy as jnp
 from jax import lax
+from jax.experimental import pallas as pl
+from jax.experimental.pallas import tpu as pltpu
 from jax.sharding import PartitionSpec as P
 
 CONV_K = 31
 GROUP = 128
-
-
+CAP = 12
 CLAMP_LIMIT = 7.0
 SLOPE_ALPHA = 1.702
+MESH = pl.DeviceIdType.MESH
+BF = jnp.bfloat16
+F32 = jnp.float32
+N_SP = 64
+N_TP = 4
+NZ = 8
+PER_Z = 8
+QW = 512
+ORDER = (0, 1, 7, 2, 6, 3, 5, 4)
+BACK = (4, 3, 5, 2, 6, 1, 7, 0)
+
+
+def coords():
+    sp = lax.axis_index("sp")
+    tp = lax.axis_index("tp")
+    return sp, tp, lax.rem(tp + 1, N_TP), lax.rem(tp + N_TP - 1, N_TP)
+
+
+def greet_all(sp, tp, right, left):
+    barrier = pltpu.get_barrier_semaphore()
+
+    def hello(i, carry):
+        pl.semaphore_signal(
+            barrier, inc=1, device_id=(lax.rem(sp + i, N_SP), tp), device_id_type=MESH
+        )
+        return carry
+
+    lax.fori_loop(1, N_SP, hello, 0)
+    pl.semaphore_signal(barrier, inc=1, device_id=(sp, right), device_id_type=MESH)
+    pl.semaphore_signal(barrier, inc=1, device_id=(sp, left), device_id_type=MESH)
+    pl.semaphore_wait(barrier, N_SP + 1)
+
+
+def remote(src, dst, send, recv, device):
+    return pltpu.make_async_remote_copy(
+        src_ref=src, dst_ref=dst, send_sem=send, recv_sem=recv, device_id=device, device_id_type=MESH
+    )
+
+
+def columns(quarter):
+    return pl.ds(pl.multiple_of(quarter * QW, QW), QW)
+
+
+def dispatch_kernel(send_ref, out_ref, a_send, a_recv, x_send, x_recv, r_recv, own_sem):
+    sp, tp, right, left = coords()
+    z = sp // PER_Z
+    mine, from_left, from_right = columns(tp), columns(left), columns(right)
+    own = pltpu.make_async_copy(send_ref.at[:, sp], out_ref.at[:, sp, :, mine], own_sem)
+    own.start()
+    greet_all(sp, tp, right, left)
+
+    def to_peer(peer):
+        return remote(
+            send_ref.at[:, peer], out_ref.at[:, sp, :, mine], a_send, a_recv.at[z], (peer, tp)
+        )
+
+    for dz in ORDER:
+        target = lax.rem(z + dz, NZ) * PER_Z
+
+        def send_one(m, carry):
+            to_peer(target + lax.rem(sp + m, PER_Z)).start()
+            return carry
+
+        lax.fori_loop(1 if dz == 0 else 0, PER_Z, send_one, 0)
+
+    def group(zs, cols, first=0, count=PER_Z):
+        return out_ref.at[:, pl.ds(zs * PER_Z + first, count), :, cols]
+
+    def relay(zs):
+        half = PER_Z // 2
+        remote(group(zs, from_left), group(zs, from_left), x_send, x_recv.at[0, zs], (sp, right)).wait_recv()
+        remote(group(zs, from_left, 0, half), group(zs, from_left, 0, half), x_send, r_recv.at[0, zs], (sp, right)).start()
+        remote(group(zs, from_right), group(zs, from_right), x_send, x_recv.at[1, zs], (sp, left)).wait_recv()
+        remote(group(zs, from_right, half, half), group(zs, from_right, half, half), x_send, r_recv.at[1, zs], (sp, left)).start()
+
+    own.wait()
+    previous = None
+    for dz in ORDER:
+        zs = lax.rem(z + NZ - dz, NZ)
+        arrived = group(zs, mine, 0, PER_Z - 1 if dz == 0 else PER_Z)
+        remote(arrived, arrived, a_send, a_recv.at[zs], (sp, right)).wait_recv()
+        block = group(zs, mine)
+        remote(block, block, x_send, x_recv.at[0, zs], (sp, right)).start()
+        remote(block, block, x_send, x_recv.at[1, zs], (sp, left)).start()
+        if previous is not None:
+            relay(previous)
+        previous = zs
+    relay(previous)
+    far = columns(lax.rem(tp + 2, N_TP))
+    for dz in ORDER:
+        zs = lax.rem(z + NZ - dz, NZ)
+        half = PER_Z // 2
+        a, b = group(zs, far, 0, half), group(zs, far, half, half)
+        remote(a, a, x_send, r_recv.at[0, zs], (sp, right)).wait_recv()
+        remote(b, b, x_send, r_recv.at[1, zs], (sp, left)).wait_recv()
+        block = group(zs, mine)
+        for _ in range(3):
+            remote(block, block, x_send, x_recv.at[0, zs], (sp, right)).wait_send()
+    sent = send_ref.at[:, pl.ds(0, N_SP - 1)]
+    remote(sent, sent, a_send, a_recv.at[0], (sp, right)).wait_send()
+
+
+def dispatch(send):
+    return pl.pallas_call(
+        dispatch_kernel,
+        out_shape=jax.ShapeDtypeStruct((3, N_SP, 8, N_TP * QW), BF),
+        in_specs=[pl.BlockSpec(memory_space=pl.ANY)],
+        out_specs=pl.BlockSpec(memory_space=pl.ANY),
+        scratch_shapes=[
+            pltpu.SemaphoreType.DMA,
+            pltpu.SemaphoreType.DMA((NZ,)),
+            pltpu.SemaphoreType.DMA,
+            pltpu.SemaphoreType.DMA((2, NZ)),
+            pltpu.SemaphoreType.DMA((2, NZ)),
+            pltpu.SemaphoreType.DMA,
+        ],
+        compiler_params=pltpu.CompilerParams(collective_id=0, has_side_effects=True),
+        name="dispatch",
+    )(send)
+
+
+TILES = 12
+HALF = TILES // 2
+
+
+def return_kernel(
+    part_ref, out_ref, opp, near, stage, rows, o_send, o_recv, n_send, n_recv, b_send, b_recv, own_sem
+):
+    sp, tp, right, left = coords()
+    z = sp // PER_Z
+    member = lax.rem(sp, PER_Z)
+    greet_all(sp, tp, right, left)
+    far = columns(lax.rem(tp + 2, N_TP))
+    sides = ((0, right, left, 0), (1, left, right, HALF))
+
+    def opposite(side, zs):
+        _, ahead, _, first = sides[side]
+        return remote(
+            part_ref.at[zs, pl.ds(first, HALF), :, far],
+            opp.at[side, zs],
+            o_send,
+            o_recv.at[side, zs],
+            (sp, ahead),
+        )
+
+    def onward(side, zs):
+        return remote(
+            stage.at[side, zs], near.at[side, zs], n_send, n_recv.at[side, zs], (sp, sides[side][1])
+        )
+
+    def home(zs):
+        for side in (0, 1):
+            onward(side, zs).wait_recv()
+        total = part_ref[zs, :, :, columns(tp)].astype(F32)
+        total = total + near[0, zs].astype(F32) + near[1, zs].astype(F32)
+        rows[zs] = total.astype(BF)
+
+        def tiles(m):
+            return ((m, 0), (PER_Z + m // 2, 1))
+
+        def send_one(m, carry):
+            for tile, kind in tiles(m):
+                remote(rows.at[zs, tile], out_ref.at[kind, sp], b_send, b_recv, (zs * PER_Z + m, tp)).start()
+            return carry
+
+        return send_one, tiles
+
+    order = [lax.rem(z + dz, NZ) for dz in BACK]
+    for zs in order:
+        for side in (0, 1):
+            opposite(side, zs).start()
+    for k, zs in enumerate(order + [None]):
+        if zs is not None:
+            for side in (0, 1):
+                _, ahead, _, first = sides[side]
+                opposite(side, zs).wait_recv()
+                other = HALF - first
+                stage[side, zs, pl.ds(first, HALF)] = (
+                    part_ref[zs, pl.ds(first, HALF), :, columns(ahead)].astype(F32)
+                    + opp[side, zs].astype(F32)
+                ).astype(BF)
+                stage[side, zs, pl.ds(other, HALF)] = part_ref[zs, pl.ds(other, HALF), :, columns(ahead)]
+                onward(side, zs).start()
+        if k > 0:
+            prev = order[k - 1]
+            send_one, tiles = home(prev)
+            if BACK[k - 1] != 0:
+                lax.fori_loop(0, PER_Z, send_one, 0)
+            else:
+                lax.fori_loop(1, PER_Z, lambda i, c: send_one(lax.rem(member + i, PER_Z), c), 0)
+                for tile, kind in tiles(member):
+                    pltpu.make_async_copy(rows.at[prev, tile], out_ref.at[kind, sp], own_sem).start()
+    mine = out_ref.at[:, pl.ds(0, 1)]
+    pltpu.make_async_copy(mine, mine, own_sem).wait()
+    for zs in order:
+        for side in (0, 1):
+            opposite(side, zs).wait_send()
+            onward(side, zs).wait_send()
+    rest = out_ref.at[:, pl.ds(0, N_SP - 1)]
+    everything = remote(rest, rest, b_send, b_recv, (sp, right))
+    everything.wait_recv()
+    everything.wait_send()
+
+
+def send_back(part):
+    return pl.pallas_call(
+        return_kernel,
+        out_shape=jax.ShapeDtypeStruct((2, N_SP, 8, QW), BF),
+        in_specs=[pl.BlockSpec(memory_space=pltpu.VMEM)],
+        out_specs=pl.BlockSpec(memory_space=pltpu.VMEM),
+        scratch_shapes=[
+            pltpu.VMEM((2, NZ, HALF, 8, QW), BF),
+            pltpu.VMEM((2, NZ, TILES, 8, QW), BF),
+            pltpu.VMEM((2, NZ, TILES, 8, QW), BF),
+            pltpu.VMEM((NZ, TILES, 8, QW), BF),
+            pltpu.SemaphoreType.DMA,
+            pltpu.SemaphoreType.DMA((2, NZ)),
+            pltpu.SemaphoreType.DMA,
+            pltpu.SemaphoreType.DMA((2, NZ)),
+            pltpu.SemaphoreType.DMA,
+            pltpu.SemaphoreType.DMA,
+            pltpu.SemaphoreType.DMA,
+        ],
+        compiler_params=pltpu.CompilerParams(collective_id=1, has_side_effects=True),
+        name="send_back",
+    )(part)
 
 
 def sent_to_all(shard, axis):
@@ -59,26 +288,38 @@
     )
 
 
-def expert_backward(routed_rows, routed_cots, w_gate, w_up, w_down):
-    gate_pre = jnp.dot(routed_rows, w_gate, preferred_element_type=jnp.float32)
-    up_pre = jnp.dot(routed_rows, w_up, preferred_element_type=jnp.float32)
+def expert_backward(arrived, w_gate, w_up, w_down):
+    width = arrived.shape[-1]
+    tall = arrived.reshape(3 * N_SP * 8, width)
+    n = N_SP * 8
+    with_rows, with_cots = tall[: 2 * n], tall[n:]
+    gate_pre = jnp.dot(with_rows, w_gate, preferred_element_type=F32)
+    up_pre = jnp.dot(with_rows, w_up, preferred_element_type=F32)
+    raw = contract_cols(with_cots, w_down)
+    act_grad = jnp.concatenate([raw[n:], jnp.roll(raw[:n], -4, axis=0)], axis=0)
+    index = lax.broadcasted_iota(jnp.int32, (2 * n, 1), 0)
+    valid = (index < n) | (index % 8 < 4)
     gate_clamped = jnp.minimum(gate_pre, CLAMP_LIMIT)
     up_clamped = jnp.clip(up_pre, -CLAMP_LIMIT, CLAMP_LIMIT)
     sigma = jax.nn.sigmoid(SLOPE_ALPHA * gate_clamped)
     gated = gate_clamped * sigma
-    act = ((up_clamped + 1.0) * gated).astype(jnp.bfloat16)
-    down_grad = contract_rows(act, routed_cots).astype(jnp.bfloat16)
-    act_grad = contract_cols(routed_cots, w_down)
-    inside = (up_pre > -CLAMP_LIMIT) & (up_pre < CLAMP_LIMIT)
-    up_pre_grad = jnp.where(inside, act_grad * gated, 0.0).astype(jnp.bfloat16)
+    act = jnp.where(valid, (up_clamped + 1.0) * gated, 0.0)
+    inside = valid & (up_pre > -CLAMP_LIMIT) & (up_pre < CLAMP_LIMIT)
+    up_pre_grad = jnp.where(inside, act_grad * gated, 0.0).astype(BF)
     slope = sigma + SLOPE_ALPHA * gate_clamped * sigma * (1.0 - sigma)
     gate_pre_grad = jnp.where(
-        gate_pre < CLAMP_LIMIT, act_grad * (up_clamped + 1.0) * slope, 0.0
-    ).astype(jnp.bfloat16)
-    gate_grad = contract_rows(routed_rows, gate_pre_grad).astype(jnp.bfloat16)
-    up_grad = contract_rows(routed_rows, up_pre_grad).astype(jnp.bfloat16)
-    partial_value = contract_cols(gate_pre_grad, w_gate) + contract_cols(up_pre_grad, w_up)
-    return (gate_grad, up_grad, down_grad, partial_value)
+        valid & (gate_pre < CLAMP_LIMIT), act_grad * (up_clamped + 1.0) * slope, 0.0
+    ).astype(BF)
+    act_placed = jnp.concatenate([jnp.roll(act[n:], 4, axis=0), act[:n]], axis=0).astype(BF)
+    partial = contract_cols(gate_pre_grad, w_gate) + contract_cols(up_pre_grad, w_up)
+    part_a = partial[:n].astype(BF).reshape(NZ, PER_Z, 8, width)
+    part_b = partial[n:].reshape(NZ, PER_Z // 2, 2, 8, width)
+    packed = jnp.concatenate([part_b[:, :, 0, :4], part_b[:, :, 1, :4]], axis=2).astype(BF)
+    back = jnp.concatenate([part_a, packed], axis=1)
+    down_grad = contract_rows(act_placed, with_cots).astype(BF)
+    gate_grad = contract_rows(with_rows, gate_pre_grad).astype(BF)
+    up_grad = contract_rows(with_rows, up_pre_grad).astype(BF)
+    return gate_grad, up_grad, down_grad, back
 
 
 def local(
@@ -98,56 +339,52 @@
     conv_gate,
 ):
     tok_rows, model_width = resid.shape
-    sp_count = lax.axis_size("sp")
-    tp_count = lax.axis_size("tp")
-    capacity = 3 * tok_rows // sp_count
-    col_count = model_width // tp_count
-    resid_f = resid.astype(jnp.float32)
+    tp = lax.axis_index("tp")
+    core = lax.axis_index("sp") % 2
+    resid_f = resid.astype(F32)
     inv_rms = lax.rsqrt(jnp.mean(resid_f * resid_f, axis=-1, keepdims=True) + 1e-06)
-    normed = (resid_f * inv_rms * norm_gain).astype(jnp.bfloat16)
-    scaled = (route_weights[:, :, None] * grad_out.astype(jnp.float32)[:, None, :]).astype(
-        jnp.bfloat16
-    )
-    scaled = scaled.reshape(2 * tok_rows, model_width)
-    route_ids = routes.reshape(-1)
-    one_hot = (route_ids[:, None] == jnp.arange(sp_count, dtype=jnp.int32)[None, :]).astype(
-        jnp.int32
-    )
-    slot_rank = jnp.sum(jnp.cumsum(one_hot, axis=0) * one_hot, axis=1) - 1
-    slot_index = route_ids * capacity + slot_rank
-    slot_table = jnp.full((sp_count * capacity,), 2 * tok_rows, jnp.int32)
-    slot_table = slot_table.at[slot_index].set(jnp.arange(2 * tok_rows, dtype=jnp.int32))
-    normed_pad = jnp.concatenate([normed, jnp.zeros((1, model_width), jnp.bfloat16)], axis=0)
-    scaled_pad = jnp.concatenate([scaled, jnp.zeros((1, model_width), jnp.bfloat16)], axis=0)
-    first_col = lax.axis_index("tp") * col_count
-    normed_part = lax.dynamic_slice_in_dim(normed_pad, first_col, col_count, 1)
-    scaled_part = lax.dynamic_slice_in_dim(scaled_pad, first_col, col_count, 1)
-    send_rows = normed_part[slot_table // 2].reshape(sp_count, capacity, col_count)
-    send_cots = scaled_part[slot_table].reshape(sp_count, capacity, col_count)
-    part_rows, part_cots = (
-        lax.all_to_all(send_rows, "sp", split_axis=0, concat_axis=0, tiled=True),
-        lax.all_to_all(send_cots, "sp", split_axis=0, concat_axis=0, tiled=True),
-    )
-    routed_rows, routed_cots = (
-        lax.all_gather(part_rows, "tp", axis=2, tiled=True),
-        lax.all_gather(part_cots, "tp", axis=2, tiled=True),
-    )
-    routed_rows = routed_rows.reshape(sp_count * capacity, model_width)
-    routed_cots = routed_cots.reshape(sp_count * capacity, model_width)
-    gate_grad, up_grad, down_grad, partial_value = expert_backward(
-        routed_rows, routed_cots, gate_weight[0], up_weight[0], down_weight[0]
-    )
-    row_grad = lax.psum_scatter(
-        partial_value.reshape(sp_count, capacity, model_width).astype(jnp.bfloat16),
-        "tp",
-        scatter_dimension=2,
-        tiled=True,
-    )
-    returned = lax.all_to_all(row_grad, "sp", split_axis=0, concat_axis=0, tiled=True).reshape(
-        sp_count * capacity, col_count
-    )
-    normed_part_grad = returned[slot_index].reshape(tok_rows, 2, col_count).astype(jnp.float32)
-    normed_part_grad = normed_part_grad.sum(axis=1).astype(jnp.bfloat16)
+    first_col = tp * QW
+    resid_q = lax.dynamic_slice_in_dim(resid, first_col, QW, 1).astype(F32)
+    gain_q = lax.dynamic_slice_in_dim(norm_gain, first_col, QW, 0)
+    normed_q = (resid_q * inv_rms * gain_q).astype(BF)
+    grad_q = lax.dynamic_slice_in_dim(grad_out, first_col, QW, 1)
+
+    experts = lax.broadcasted_iota(jnp.int32, (N_SP, tok_rows), 0)
+    hit0 = routes[:, 0][None, :] == experts
+    hit1 = routes[:, 1][None, :] == experts
+    named = hit0 | hit1
+    weight_of = jnp.where(hit0, route_weights[:, 0][None, :], 0.0) + jnp.where(
+        hit1, route_weights[:, 1][None, :], 0.0
+    )
+    earlier = (
+        lax.broadcasted_iota(jnp.int32, (tok_rows, tok_rows), 0)
+        < lax.broadcasted_iota(jnp.int32, (tok_rows, tok_rows), 1)
+    ).astype(BF)
+    rank = jnp.dot(named.astype(BF), earlier, preferred_element_type=F32).astype(jnp.int32)
+    rank = jnp.where(named, rank, -1)
+    lane8 = jnp.arange(8, dtype=jnp.int32)[None, :, None]
+    slot_a = rank[:, None, :] == lane8
+    slot_b = rank[:, None, :] == 8 + lane8 % 4
+    slots = jnp.stack([slot_a, slot_b], axis=0)
+    slot_weight = jnp.sum(jnp.where(slots, weight_of[None, :, None, :], 0.0), axis=-1, keepdims=True)
+    chosen = slots.astype(BF).reshape(2 * N_SP * 8, tok_rows)
+    picked_rows = jnp.dot(chosen, normed_q, preferred_element_type=F32).astype(BF)
+    picked_cots = (
+        slot_weight.reshape(2 * N_SP * 8, 1) * jnp.dot(chosen, grad_q, preferred_element_type=F32)
+    ).astype(BF)
+    n = N_SP * 8
+    lower = (lax.broadcasted_iota(jnp.int32, (n, 1), 0) % 8) < 4
+    mixed = jnp.where(lower, picked_rows[n:], picked_cots[n:])
+    send = jnp.concatenate([picked_rows[:n], mixed, picked_cots[:n]], axis=0).reshape(3, N_SP, 8, QW)
+    arrived = dispatch(send)
+    gate_grad, up_grad, down_grad, back = expert_backward(
+        arrived, gate_weight[0], up_weight[0], down_weight[0]
+    )
+    returned = send_back(back)
+    returned = returned.reshape(2 * n, QW)
+    owner = lane8 // 4 == core
+    back_slots = jnp.stack([slot_a, slot_b & owner], axis=0).astype(BF).reshape(2 * n, tok_rows)
+    normed_part_grad = contract_rows(back_slots, returned).astype(BF)
     normed_grad = collect(normed_part_grad, "tp", 1)
     feature_grad = normed_grad.astype(jnp.float32) * norm_gain
     cubed = inv_rms * inv_rms * inv_rms

time: 339 us -> 214 us (0.63)
  Pallas kernels: 0 us -> 123 us
  waiting for transfers between devices: 123 us -> 6.92 us
  blocking collectives: 76.1 us -> 0 us
  local copies, waits for them, and re-layouts: 52.4 us -> 16.4 us
  between operations: 14.3 us -> 1.17 us
  starting transfers between devices: 24.7 us -> 16.2 us
  matrix products: 35.3 us -> 39.9 us
    pallas_call x0 -> x2, Pallas kernels: none -> 123 us  [the longest x1 77.3 us: dispatch(): pl.pallas_call(dispatch_kernel, out_shape=jax.ShapeDtypeStruct((3, N_SP,...]
    all_to_all x2 -> x0, blocking collectives: 76.1 us -> none  [the longest x1 41.4 us: local(): lax.all_to_all(send_rows, 'sp', split_axis=0, concat_axis=0, tiled=True)]
    reduce_scatter x1 -> x0, waiting for transfers between devices: 50 us -> none  [local(): lax.psum_scatter(partial_value.reshape(sp_count, capacity, model_width).a...]
    all_gather x2 -> x0, waiting for transfers between devices: 32.9 us -> none  [the longest x1 32.9 us: local(): lax.all_gather(part_cots, 'tp', axis=2, tiled=True)]
    all_to_all x1 -> x0, waiting for transfers between devices: 27.7 us -> none  [local(): lax.all_to_all(row_grad, 'sp', split_axis=0, concat_axis=0, tiled=True)]
    reshape x6 -> x0, local copies, waits for them, and re-layouts: 18 us -> none  [the longest x1 6.17 us: local(): routed_rows = routed_rows.reshape(sp_count * capacity, model_width)]
    mul x5 -> x1, local copies, waits for them, and re-layouts: 12 us -> 0.09 us  [local(): slot_weight.reshape(2 * N_SP * 8, 1)]
    all_to_all x1 -> x0, starting transfers between devices: 11 us -> none  [local(): lax.all_to_all(row_grad, 'sp', split_axis=0, concat_axis=0, tiled=True)]
  transfers between devices with their start and end apart: 7 -> 3, of which waited for: 5 -> 2; matrix products, arithmetic and copies ran while one was open for 15% -> 10% of each run, Pallas kernels for 0% -> 0%
where the time goes in v1:
time: 214 us; the launch traced here: 213 us
  Pallas kernels  123 us (57%)
  matrix products  39.9 us (19%)
  local copies, waits for them, and re-layouts  16.4 us (8%)
  starting transfers between devices  16.2 us (8%)
  other arithmetic  9.48 us (4%)
  waiting for transfers between devices  6.92 us (3%)
    pallas_call x1, Pallas kernels, dispatch(): pl.pallas_call(dispatch_kernel, out_shape=jax.ShapeDtypeStruct((3, N_SP,...  77.3 us
    pallas_call x1, Pallas kernels, send_back(): pl.pallas_call(return_kernel, out_shape=jax.ShapeDtypeStruct((2, N_SP, 8,...  45.7 us
    dot_general x5, matrix products, contract_rows(): lax.dot_general(left_side, right_side, (((0,), (0,)), ((), ())), preferre...  19.8 us
    all_to_all x1, starting transfers between devices, summed_on_arrival(): lax.all_to_all(parts, axis, split_axis=0, concat_axis=0, tiled=True)  9.35 us
    dot_general x3, matrix products, contract_cols(): lax.dot_general(left_side, right_side, (((1,), (1,)), ((), ())), preferre...  7.11 us
    all_to_all x1, waiting for transfers between devices, summed_on_arrival(): lax.all_to_all(parts, axis, split_axis=0, concat_axis=0, tiled=True)  6.41 us
    unnamed x44, local copies, waits for them, and re-layouts  5.79 us
    dot_general x1, matrix products, expert_backward(): up_pre = jnp.dot(with_rows, w_up, preferred_element_type=F32)  5.45 us
  transfers between devices with their start and end apart: 3, of which 2 were waited for; matrix products, arithmetic and copies ran while one was open for 10% of the time, Pallas kernels for 0%

profile of v1, /device:TPU:1, one launch (start us, length us, event | category | flops | bytes accessed | tf_op | source)
XLA Modules:
  0.0 213.1 jit_solution(17485649144202201383)
XLA Ops:
  0.6 0.0 copy-start
  0.7 0.8 fusion.89
  1.5 0.8 fusion.88
  2.3 0.2 fusion.20
  2.5 0.8 broadcast_and_fusion
  3.3 0.3 select_reduce_fusion
  3.6 0.2 copy.42
  3.8 1.5 copy.43
  5.3 0.3 fusion.3
  5.6 0.1 copy.44
  5.7 0.1 mul.185
  5.8 0.1 dynamic_slice.10
  5.9 1.5 convolution_convert_fusion.4
  7.4 1.4 multiply_convert_fusion
  8.8 0.2 fusion.87
  9.0 1.2 pad_maximum_fusion
  10.3 77.3 %dispatch.1 = bf16[3,64,8,2048]{3,2,1,0:T(8,128)(2,1)} custom-call(bf16[3,64,8,512]{3,2,1,0:T(8,128)(2,1)} %bitcast.83), custom_call_target="tpu_custom_call" | custom-call | tf_op jit(solution)/shard_map/dispatch/pallas_call | solution.py:118
  87.6 0.0 copy-start.17
  87.7 4.1 %fusion.85 = (bf16[2,64,8,2048]{3,2,1,0:T(8,128)(2,1)S(1)}, bf16[2,64,8,2048]{3,2,1,0:T(8,128)(2,1)S(1)}) fusion(bf16[3,64,8,2048]{3,2,1,0:T(8,128)(2,1)} %dispatch.1), kind=kLoop, calls=%fused_computation.149 | loop fusion | bytes 16777216 | tf_op jit(solution)/shard_map/slice | solution.py:295
  91.8 2.3 %fusion.11 = f32[1024,384]{1,0:T(8,128)S(1)} fusion(bf16[1024,2048]{1,0:T(8,128)(2,1)S(1)} %bitcast.85, bf16[1,384,2048]{2,1,0:T(8,128)(2,1)S(1)} %copy-done.17), kind=kOutput, calls=%fused_computation.26 | convolution fusion | flops 1610612736 | bytes 7340032 | tf_op jit(solution)/shard_map/dot_general | solution.py:286
  94.2 0.0 copy-start.4
  94.2 0.1 slice.117
  94.2 0.1 slice.116
  94.3 1.5 copy-done.4
  95.9 2.3 %fusion.15 = f32[1024,384]{1,0:T(8,128)S(1)} fusion(bf16[1024,2048]{1,0:T(8,128)(2,1)S(1)} %bitcast.87, bf16[1,2048,384]{2,1,0:T(8,128)(2,1)S(1)} %copy-done.4), kind=kOutput, calls=%fused_computation.30 | convolution fusion | flops 1610612736 | bytes 7340032 | tf_op jit(solution)/shard_map/dot_general | solution.py:296
  98.2 5.4 %select_convert_fusion.1 = (bf16[1024,384]{1,0:T(8,128)(2,1)S(1)}, bf16[1024,384]{1,0:T(8,128)(2,1)S(1)}, bf16[1024,384]{1,0:T(8,128)(2,1)}) fusion(f32[4,384]{1,0:T(4,128)S(1)} %slice.118, f32[508,384]{1,0:T(8,128)S(1)} %slice.117, f32[512,384]{1,0:T(8,128)S(1)} %slice.116, pred[1024]{0:T(1024)(128)(4,1)S(1)} %fusion.68, f32[1024,384]{1,0:T(8,128)S(1)} %fusion.15, ...), kind=kOutput, calls=%fused_computation.33 | convolution fusion | flops 1622409216 | bytes 11273216 | tf_op jit(solution)/shard_map/dot_general | solution.py:297
  103.7 2.4 %fusion.13 = f32[1024,2048]{1,0:T(8,128)S(1)} fusion(bf16[1024,384]{1,0:T(8,128)(2,1)S(1)} %get-tuple-element.13, bf16[1,2048,384]{2,1,0:T(8,128)(2,1)S(1)} %copy-done.4), kind=kOutput, calls=%fused_computation.28 | convolution fusion | flops 1610612736 | bytes 10747904 | tf_op jit(solution)/shard_map/dot_general | solution.py:286
  106.1 2.4 %convolution_add_fusion = bf16[1024,2048]{1,0:T(8,128)(2,1)S(1)} fusion(f32[1024,2048]{1,0:T(8,128)S(1)} %fusion.13, bf16[1024,384]{1,0:T(8,128)(2,1)S(1)} %get-tuple-element.12, bf16[1,2048,384]{2,1,0:T(8,128)(2,1)S(1)} %copy-done), kind=kOutput, calls=%fused_computation | convolution fusion | flops 1614807040 | bytes 14942208 | tf_op jit(solution)/shard_map/dot_general | solution.py:286
  108.4 0.3 fusion.86
  108.8 0.5 slice_bitcast_fusion.1
  109.3 2.2 %maximum_maximum_fusion.part_ref = bf16[8,12,8,2048]{3,2,1,0:T(8,128)(2,1)} fusion(bf16[8,4,4,2048]{3,2,1,0:T(4,128)(2,1)S(1)} %get-tuple-element.18, bf16[8,4,4,2048]{3,2,1,0:T(4,128)(2,1)S(1)} %get-tuple-element.17, bf16[8,8,8,2048]{3,2,1,0:T(8,128)(2,1)S(1)} %bitcast.82), kind=kLoop, calls=%fused_computation.3 | loop fusion | flops 9437184 | bytes 6291456 | tf_op jit(solution)/shard_map/concatenate | solution.py:318
  111.6 45.7 %send_back.1 = bf16[2,64,8,512]{3,2,1,0:T(8,128)(2,1)} custom-call(bf16[8,12,8,2048]{3,2,1,0:T(8,128)(2,1)} %maximum_maximum_fusion.part_ref), custom_call_target="tpu_custom_call" | custom-call | tf_op jit(solution)/shard_map/send_back/pallas_call | solution.py:220
  157.3 1.8 fusion.17
  159.1 1.0 broadcast_in_dim.107
  160.1 4.5 %all-to-all-start = ((bf16[4,256,512]{2,1,0:T(8,128)(2,1)}), bf16[4,256,512]{2,1,0:T(8,128)(2,1)}, u32[]{:S(2)}, u32[]{:S(2)}) async-start(bf16[4,256,512]{2,1,0:T(8,128)(2,1)} %broadcast_in_dim.107), calls=%async_computation | async-start | bytes 2097152 | tf_op jit(solution)/shard_map/all_to_all | solution.py:245
  164.6 0.0 copy-start.10
  164.6 0.0 copy-start.7
  164.6 5.8 %fusion = bf16[1,2048,384]{2,1,0:T(8,128)(2,1)} fusion(bf16[1024,2048]{1,0:T(8,128)(2,1)} %bitcast.89, bf16[1024,384]{1,0:T(8,128)(2,1)S(1)} %get-tuple-element.13), kind=kOutput, calls=%fused_computation.10 | convolution fusion | flops 1611399168 | bytes 6553600 | tf_op jit(solution)/shard_map/dot_general | solution.py:280
  170.4 0.1 convert_reduce_fusion.1
  170.5 0.2 fusion.54
  170.8 0.8 slice.120
  171.6 0.0 copy-done.5
  171.6 1.3 copy.45
  173.0 5.7 %fusion.1 = bf16[1,2048,384]{2,1,0:T(8,128)(2,1)} fusion(bf16[1024,2048]{1,0:T(8,128)(2,1)} %bitcast.90, bf16[1024,384]{1,0:T(8,128)(2,1)S(1)} %copy-done.9), kind=kOutput, calls=%fused_computation.11 | convolution fusion | flops 1611399168 | bytes 6553600 | tf_op jit(solution)/shard_map/dot_general | solution.py:280
  178.7 0.5 all-to-all-done
  179.2 1.5 copy.49
  180.7 0.4 fusion.7
  181.1 0.0 copy-start.19
  181.1 1.9 fusion.6
  183.1 1.0 copy-done.6
  184.0 1.3 convolution_convert_fusion.3
  185.4 9.4 %all-to-all-start.1 = ((bf16[64,32,128]{2,1,0:T(8,128)(2,1)}), bf16[64,32,128]{2,1,0:T(8,128)(2,1)S(1)}, u32[]{:S(2)}, u32[]{:S(2)}) async-start(bf16[64,32,128]{2,1,0:T(8,128)(2,1)} %bitcast.22), calls=%async_computation.1 | async-start | bytes 1048576 | tf_op jit(solution)/shard_map/all_to_all | solution.py:269
  194.7 1.8 fusion.84
  196.6 0.2 fusion.53
  196.8 0.0 copy-start.20
  196.8 2.4 %collective-permute-start = (f32[30,128]{1,0:T(8,128)S(1)}, f32[30,128]{1,0:T(8,128)S(1)}, u32[]{:S(2)}, u32[]{:S(2)}) collective-permute-start(f32[30,128]{1,0:T(8,128)S(1)} %slice.126), channel_id=1, source_target_pairs={{4,0},{8,4},{12,8},{16,12},{20,16},{24,20},{28,24},{32,28},{36,32}... | collective-permute-start | bytes 46088 | tf_op jit(solution)/shard_map/ppermute | solution.py:276
  199.2 5.2 %fusion.2 = bf16[1,384,2048]{2,1,0:T(8,128)(2,1)} fusion(bf16[1024,2048]{1,0:T(8,128)(2,1)} %bitcast.86, bf16[512,384]{1,0:T(8,128)(2,1)S(1)} %slice.121, bf16[508,384]{1,0:T(8,128)(2,1)S(1)} %copy-done.11, bf16[4,384]{1,0:T(4,128)(2,1)S(1)} %slice.119), kind=kOutput, calls=%fused_computation.12 | convolution fusion | flops 1613758464 | bytes 6553600 | tf_op jit(solution)/shard_map/dot_general | solution.py:280
  204.4 0.0 copy-start.13
  204.5 0.4 convolution_select_fusion
  204.9 0.3 copy-done.13
  205.3 0.0 copy-done.14
  205.3 0.7 multiply_convert_fusion.3
  206.0 6.4 %all-to-all-done.1 = bf16[64,32,128]{2,1,0:T(8,128)(2,1)S(1)} async-done(((bf16[64,32,128]{2,1,0:T(8,128)(2,1)}), bf16[64,32,128]{2,1,0:T(8,128)(2,1)S(1)}, u32[]{:S(2)}, u32[]{:S(2)}) %all-to-all-start.1) | async-done | bytes 524320 | tf_op jit(solution)/shard_map/all_to_all | solution.py:269
  212.4 0.7 convert_reduce_fusion
  (51 shorter events, 0.3 us)
Async XLA Ops:
  0.6 97.6 %copy-start = (bf16[1,2048,384]{2,1,0:T(8,128)(2,1)S(1)}, bf16[1,2048,384]{2,1,0:T(8,128)(2,1)}, u32[]{:S(2)}) copy-start(bf16[1,2048,384]{2,1,0:T(8,128)(2,1)} %param.20) | copy-start | bytes 4718596
  3.3 2.5 %copy-start.15 = (f32[2048]{0:T(1024)S(1)}, f32[2048]{0:T(1024)}, u32[]{:S(2)}) copy-start(f32[2048]{0:T(1024)} %param.16) | copy-start | bytes 24580
  87.6 4.1 %copy-start.17 = (bf16[1,384,2048]{2,1,0:T(8,128)(2,1)S(1)}, bf16[1,384,2048]{2,1,0:T(8,128)(2,1)}, u32[]{:S(2)}) copy-start(bf16[1,384,2048]{2,1,0:T(8,128)(2,1)} %param.21) | copy-start | bytes 4718596
  91.8 2.4 %copy-start.2 = (bf16[2,64,8,2048]{3,2,1,0:T(8,128)(2,1)}, bf16[2,64,8,2048]{3,2,1,0:T(8,128)(2,1)S(1)}, u32[]{:S(2)}) copy-start(bf16[2,64,8,2048]{3,2,1,0:T(8,128)(2,1)S(1)} %get-tuple-element.10) | copy-start | bytes 12582916
  91.8 6.4 %copy-start.3 = (bf16[2,64,8,2048]{3,2,1,0:T(8,128)(2,1)}, bf16[2,64,8,2048]{3,2,1,0:T(8,128)(2,1)S(1)}, u32[]{:S(2)}) copy-start(bf16[2,64,8,2048]{3,2,1,0:T(8,128)(2,1)S(1)} %get-tuple-element.11) | copy-start | bytes 12582916
  94.2 1.7 copy-start.4
  103.7 2.4 %copy-start.8 = (bf16[1024,384]{1,0:T(8,128)(2,1)}, bf16[1024,384]{1,0:T(8,128)(2,1)S(1)}, u32[]{:S(2)}) copy-start(bf16[1024,384]{1,0:T(8,128)(2,1)S(1)} %get-tuple-element.12) | copy-start | bytes 2359300
  111.6 45.7 %copy-start.12 = (pred[1,64,8,256]{3,1,2,0:T(32,128)(4,1)S(1)}, pred[1,64,8,256]{3,1,2,0:T(32,128)(4,1)}, u32[]{:S(2)}) copy-start(pred[1,64,8,256]{3,1,2,0:T(32,128)(4,1)} %get-tuple-element.24) | copy-start | bytes 393220
  160.1 19.1 %all-to-all-start = ((bf16[4,256,512]{2,1,0:T(8,128)(2,1)}), bf16[4,256,512]{2,1,0:T(8,128)(2,1)}, u32[]{:S(2)}, u32[]{:S(2)}) async-start(bf16[4,256,512]{2,1,0:T(8,128)(2,1)} %broadcast_in_dim.107), calls=%async_computation | async-start | bytes 2097152 | tf_op jit(solution)/shard_map/all_to_all | solution.py:245
  164.6 5.8 %copy-start.10 = (bf16[256,128]{1,0:T(8,128)(2,1)S(1)}, bf16[256,128]{1,0:T(8,128)(2,1)}, u32[]{:S(2)}) copy-start(bf16[256,128]{1,0:T(8,128)(2,1)} %param.23) | copy-start | bytes 196612
  164.6 6.1 %copy-start.7 = (bf16[1024,384]{1,0:T(8,128)(2,1)S(1)}, bf16[1024,384]{1,0:T(8,128)(2,1)}, u32[]{:S(2)}) copy-start(bf16[1024,384]{1,0:T(8,128)(2,1)} %get-tuple-element.16) | copy-start | bytes 2359300
  170.4 1.2 copy-start.5
  170.4 2.5 %copy-start.9 = (bf16[1024,384]{1,0:T(8,128)(2,1)S(1)}, bf16[1024,384]{1,0:T(8,128)(2,1)}, u32[]{:S(2)}) copy-start(bf16[1024,384]{1,0:T(8,128)(2,1)} %copy-done.8) | copy-start | bytes 2359300
  181.1 2.9 %copy-start.19 = (f32[128]{0:T(128)S(1)}, f32[128]{0:T(128)}, u32[]{:S(2)}) copy-start(f32[128]{0:T(128)} %param.24) | copy-start | bytes 1540
  183.0 1.0 copy-start.6
  184.0 10.7 %copy-start.18 = (bf16[2048,128]{1,0:T(8,128)(2,1)S(1)}, bf16[2048,128]{1,0:T(8,128)(2,1)}, u32[]{:S(2)}) copy-start(bf16[2048,128]{1,0:T(8,128)(2,1)} %param.22) | copy-start | bytes 1572868
  185.4 13.8 %copy-start.11 = (bf16[508,384]{1,0:T(8,128)(2,1)S(1)}, bf16[508,384]{1,0:T(8,128)(2,1)}, u32[]{:S(2)}) copy-start(bf16[508,384]{1,0:T(8,128)(2,1)} %slice.120) | copy-start | bytes 1170436
  185.4 27.0 %all-to-all-start.1 = ((bf16[64,32,128]{2,1,0:T(8,128)(2,1)}), bf16[64,32,128]{2,1,0:T(8,128)(2,1)S(1)}, u32[]{:S(2)}, u32[]{:S(2)}) async-start(bf16[64,32,128]{2,1,0:T(8,128)(2,1)} %bitcast.22), calls=%async_computation.1 | async-start | bytes 1048576 | tf_op jit(solution)/shard_map/all_to_all | solution.py:269
  196.8 7.6 %copy-start.16 = (f32[31,128]{1,0:T(8,128)S(1)}, f32[31,128]{1,0:T(8,128)}, u32[]{:S(2)}) copy-start(f32[31,128]{1,0:T(8,128)} %param.25) | copy-start | bytes 47620
  196.8 7.7 %copy-start.20 = (pred[8,36]{0,1:T(8,128)(4,1)S(1)}, pred[8,36]{0,1:T(8,128)(4,1)}, u32[]{:S(2)}) copy-start(pred[8,36]{0,1:T(8,128)(4,1)} %constant.120) | copy-start | bytes 868
  196.8 7.6 %collective-permute-start = (f32[30,128]{1,0:T(8,128)S(1)}, f32[30,128]{1,0:T(8,128)S(1)}, u32[]{:S(2)}, u32[]{:S(2)}) collective-permute-start(f32[30,128]{1,0:T(8,128)S(1)} %slice.126), channel_id=1, source_target_pairs={{4,0},{8,4},{12,8},{16,12},{20,16},{24,20},{28,24},{32,28},{36,32}... | collective-permute-start | bytes 46088 | tf_op jit(solution)/shard_map/ppermute | solution.py:276
  204.4 0.8 copy-start.13
  204.4 0.9 copy-start.14
  204.5 8.6 %copy-start.1 = (bf16[1,2048,384]{2,1,0:T(8,128)(2,1)S(1)}, bf16[1,2048,384]{2,1,0:T(8,128)(2,1)}, u32[]{:S(2)}) copy-start(bf16[1,2048,384]{2,1,0:T(8,128)(2,1)} %param.20) | copy-start | bytes 4718596

commit v2 on v1

v2 whole, which is shorter than its diff:
```python
import functools

import jax
import jax.numpy as jnp
from jax import lax
from jax.experimental import pallas as pl
from jax.experimental.pallas import tpu as pltpu
from jax.sharding import PartitionSpec as P

CONV_K = 31
GROUP = 128
CAP = 12
CLAMP_LIMIT = 7.0
SLOPE_ALPHA = 1.702
MESH = pl.DeviceIdType.MESH
BF = jnp.bfloat16
F32 = jnp.float32
N_SP = 64
N_TP = 4
NZ = 8
PER_Z = 8
QW = 512
ORDER = (0, 1, 7, 2, 6, 3, 5, 4)


def coords():
    sp = lax.axis_index("sp")
    tp = lax.axis_index("tp")
    return sp, tp, lax.rem(tp + 1, N_TP), lax.rem(tp + N_TP - 1, N_TP)


def greet_all(sp, tp, right, left):
    barrier = pltpu.get_barrier_semaphore()

    def hello(i, carry):
        pl.semaphore_signal(
            barrier, inc=1, device_id=(lax.rem(sp + i, N_SP), tp), device_id_type=MESH
        )
        return carry

    lax.fori_loop(1, N_SP, hello, 0)
    pl.semaphore_signal(barrier, inc=1, device_id=(sp, right), device_id_type=MESH)
    pl.semaphore_signal(barrier, inc=1, device_id=(sp, left), device_id_type=MESH)
    pl.semaphore_wait(barrier, N_SP + 1)


def remote(src, dst, send, recv, device):
    return pltpu.make_async_remote_copy(
        src_ref=src, dst_ref=dst, send_sem=send, recv_sem=recv, device_id=device, device_id_type=MESH
    )


def columns(quarter):
    return pl.ds(pl.multiple_of(quarter * QW, QW), QW)


TILES = 12
HALF = TILES // 2
FH = 384


def order_of(k):
    odd = lax.rem(k, 2)
    return lax.rem(odd * ((k + 1) // 2) + (1 - odd) * (NZ - k // 2), NZ)


def experts_kernel(
    send_ref, wg_ref, wu_ref, wd_ref, out_ref, gg_out, ug_out, dg_out,
    arr, wg, wu, wd, gpg, upg, act, part, opp, near, stage, rows, gg, ug, dg,
    a_send, a_recv, x_send, x_recv, r_recv, own_sem, w_sem, o_send, o_recv, n_send, n_recv,
    b_send, b_recv, g_sem,
):
    sp, tp, right, left = coords()
    z = sp // PER_Z
    member = lax.rem(sp, PER_Z)
    mine, from_left, from_right = columns(tp), columns(left), columns(right)
    far = columns(lax.rem(tp + 2, N_TP))
    own = pltpu.make_async_copy(send_ref.at[:, sp], arr.at[:, sp, :, mine], own_sem)
    own.start()
    weights = [
        pltpu.make_async_copy(s, d, w_sem.at[i])
        for i, (s, d) in enumerate(((wg_ref, wg), (wu_ref, wu), (wd_ref, wd)))
    ]
    greet_all(sp, tp, right, left)
    for dz in ORDER:
        target = lax.rem(z + dz, NZ) * PER_Z

        def send_one(m, carry):
            peer = target + lax.rem(sp + m, PER_Z)
            remote(send_ref.at[:, peer], arr.at[:, sp, :, mine], a_send, a_recv.at[z], (peer, tp)).start()
            return carry

        lax.fori_loop(1 if dz == 0 else 0, PER_Z, send_one, 0)
    for copy in weights:
        copy.start()

    def group(zs, cols, first=0, count=PER_Z):
        return arr.at[:, pl.ds(zs * PER_Z + first, count), :, cols]

    def arrive(zs, count):
        block = group(zs, mine, 0, count)
        remote(block, block, a_send, a_recv.at[zs], (sp, right)).wait_recv()

    def forward(zs):
        block = group(zs, mine)
        remote(block, block, x_send, x_recv.at[0, zs], (sp, right)).start()
        remote(block, block, x_send, x_recv.at[1, zs], (sp, left)).start()

    half = PER_Z // 2

    def relay(zs):
        remote(group(zs, from_left), group(zs, from_left), x_send, x_recv.at[0, zs], (sp, right)).wait_recv()
        a = group(zs, from_left, 0, half)
        remote(a, a, x_send, r_recv.at[0, zs], (sp, right)).start()
        remote(group(zs, from_right), group(zs, from_right), x_send, x_recv.at[1, zs], (sp, left)).wait_recv()
        b = group(zs, from_right, half, half)
        remote(b, b, x_send, r_recv.at[1, zs], (sp, left)).start()

    sides = ((0, right, 0), (1, left, HALF))

    def opposite(side, zs):
        _, ahead, first = sides[side]
        return remote(
            part.at[zs, pl.ds(first, HALF), :, far], opp.at[side, zs], o_send, o_recv.at[side, zs], (sp, ahead)
        )

    def onward(side, zs):
        return remote(stage.at[side, zs], near.at[side, zs], n_send, n_recv.at[side, zs], (sp, sides[side][1]))

    def compute(zs):
        a, b = group(zs, far, 0, half), group(zs, far, half, half)
        remote(a, a, x_send, r_recv.at[0, zs], (sp, right)).wait_recv()
        remote(b, b, x_send, r_recv.at[1, zs], (sp, left)).wait_recv()
        n = PER_Z * 8
        members = pl.ds(zs * PER_Z, PER_Z)
        with_rows = arr[pl.ds(0, 2), members].reshape(2 * n, N_TP * QW)
        gate_pre = jnp.dot(with_rows, wg[...], preferred_element_type=F32)
        up_pre = jnp.dot(with_rows, wu[...], preferred_element_type=F32)
        with_cots = arr[pl.ds(1, 2), members].reshape(2 * n, N_TP * QW)
        raw = contract_cols(with_cots, wd[...])
        act_grad = jnp.concatenate([raw[n:], pltpu.roll(raw[:n], n - 4, 0)], axis=0)
        index = lax.broadcasted_iota(jnp.int32, (2 * n, FH), 0)
        valid = (index < n) | (lax.rem(index, 8) < 4)
        gate_clamped = jnp.minimum(gate_pre, CLAMP_LIMIT)
        up_clamped = jnp.clip(up_pre, -CLAMP_LIMIT, CLAMP_LIMIT)
        sigma = jax.nn.sigmoid(SLOPE_ALPHA * gate_clamped)
        gated = gate_clamped * sigma
        acted = jnp.where(valid, (up_clamped + 1.0) * gated, 0.0)
        inside = valid & (up_pre > -CLAMP_LIMIT) & (up_pre < CLAMP_LIMIT)
        up_grad = jnp.where(inside, act_grad * gated, 0.0)
        slope = sigma + SLOPE_ALPHA * gate_clamped * sigma * (1.0 - sigma)
        gate_grad = jnp.where(
            valid & (gate_pre < CLAMP_LIMIT), act_grad * (up_clamped + 1.0) * slope, 0.0
        )
        placed = jnp.concatenate([pltpu.roll(acted[n:], 4, 0), acted[:n]], axis=0)
        act[:, members] = placed.reshape(2, PER_Z, 8, FH).astype(BF)
        gpg[:, members] = gate_grad.reshape(2, PER_Z, 8, FH).astype(BF)
        upg[:, members] = up_grad.reshape(2, PER_Z, 8, FH).astype(BF)
        gate_b, up_b = gate_grad.astype(BF), up_grad.astype(BF)
        wide = 512
        for c in range(N_TP * QW // wide):
            cols = slice(c * wide, (c + 1) * wide)
            partial = contract_cols(gate_b, wg[cols]) + contract_cols(up_b, wu[cols])
            part[zs, 0:PER_Z, :, cols] = partial[:n].reshape(PER_Z, 8, wide).astype(BF)
            mixed = partial[n:].reshape(half, 2, 8, wide)
            packed = mixed[:, 0] + pltpu.roll(mixed[:, 1], 4, 1)
            part[zs, PER_Z:TILES, :, cols] = packed.astype(BF)
        for side in (0, 1):
            opposite(side, zs).start()

    def pass_on(zs):
        for side in (0, 1):
            _, ahead, first = sides[side]
            opposite(side, zs).wait_recv()
            other = HALF - first
            stage[side, zs, pl.ds(first, HALF)] = (
                part[zs, pl.ds(first, HALF), :, columns(ahead)].astype(F32) + opp[side, zs].astype(F32)
            ).astype(BF)
            stage[side, zs, pl.ds(other, HALF)] = part[zs, pl.ds(other, HALF), :, columns(ahead)]
            onward(side, zs).start()

    def home(zs, at_home):
        for side in (0, 1):
            onward(side, zs).wait_recv()
        total = part[zs, :, :, mine].astype(F32)
        total = total + near[0, zs].astype(F32) + near[1, zs].astype(F32)
        rows[zs] = total.astype(BF)

        def send_one(i, carry):
            m = lax.rem(member + i, PER_Z)
            for tile, kind in ((m, 0), (PER_Z + m // 2, 1)):
                remote(rows.at[zs, tile], out_ref.at[kind, sp], b_send, b_recv, (zs * PER_Z + m, tp)).start()
            return carry

        if at_home:
            for tile, kind in ((member, 0), (PER_Z + member // 2, 1)):
                pltpu.make_async_copy(rows.at[zs, tile], out_ref.at[kind, sp], g_sem).start()
        lax.fori_loop(1 if at_home else 0, PER_Z, send_one, 0)

    def source(k):
        return lax.rem(z + NZ - order_of(k), NZ)

    def step(k, carry):
        @pl.when(k == 0)
        def _():
            own.wait()
            arrive(z, PER_Z - 1)
            forward(z)

        @pl.when((k > 0) & (k < NZ))
        def _():
            zs = source(k)
            arrive(zs, PER_Z)
            forward(zs)

        @pl.when((k >= 1) & (k <= NZ))
        def _():
            relay(source(k - 1))

        @pl.when(k == 2)
        def _():
            for copy in weights:
                copy.wait()

        @pl.when((k >= 2) & (k <= NZ + 1))
        def _():
            compute(source(k - 2))

        @pl.when((k >= 3) & (k <= NZ + 2))
        def _():
            pass_on(source(k - 3))

        @pl.when(k == 4)
        def _():
            home(z, True)

        @pl.when(k >= 5)
        def _():
            home(source(k - 4), False)

        return carry

    lax.fori_loop(0, NZ + 4, step, 0)

    n = N_SP * 8
    wide = 256
    outs = [pltpu.make_async_copy(s, d, own_sem) for s, d in ((gg, gg_out), (ug, ug_out), (dg, dg_out))]

    def weight_grads(c, carry):
        cols = pl.ds(pl.multiple_of(c * wide, wide), wide)
        lhs = arr[pl.ds(0, 2), :, :, cols].reshape(2 * n, wide)
        gg[cols] = contract_rows(lhs, gpg[...].reshape(2 * n, FH)).astype(BF)
        ug[cols] = contract_rows(lhs, upg[...].reshape(2 * n, FH)).astype(BF)
        rhs = arr[pl.ds(1, 2), :, :, cols].reshape(2 * n, wide)
        dg[:, cols] = contract_rows(act[...].reshape(2 * n, FH), rhs).astype(BF)
        return carry

    lax.fori_loop(0, N_TP * QW // wide, weight_grads, 0)
    for copy in outs:
        copy.start()

    two = out_ref.at[:, pl.ds(0, 1)]
    pltpu.make_async_copy(two, two, g_sem).wait()

    def drain(zs, carry):
        block = group(zs, mine)
        for _ in range(3):
            remote(block, block, x_send, x_recv.at[0, zs], (sp, right)).wait_send()
        for side in (0, 1):
            opposite(side, zs).wait_send()
            onward(side, zs).wait_send()
        return carry

    lax.fori_loop(0, NZ, drain, 0)
    sent = send_ref.at[:, pl.ds(0, N_SP - 1)]
    remote(sent, sent, a_send, a_recv.at[0], (sp, right)).wait_send()
    for copy in outs:
        copy.wait()
    rest = out_ref.at[:, pl.ds(0, N_SP - 1)]
    everything = remote(rest, rest, b_send, b_recv, (sp, right))
    everything.wait_recv()
    everything.wait_send()


def run_experts(send, w_gate, w_up, w_down):
    width = N_TP * QW
    any_spec = pl.BlockSpec(memory_space=pl.ANY)
    return pl.pallas_call(
        experts_kernel,
        out_shape=(
            jax.ShapeDtypeStruct((2, N_SP, 8, QW), BF),
            jax.ShapeDtypeStruct((width, FH), BF),
            jax.ShapeDtypeStruct((width, FH), BF),
            jax.ShapeDtypeStruct((FH, width), BF),
        ),
        in_specs=[any_spec] * 4,
        out_specs=(pl.BlockSpec(memory_space=pltpu.VMEM), any_spec, any_spec, any_spec),
        scratch_shapes=[
            pltpu.VMEM((3, N_SP, 8, width), BF),
            pltpu.VMEM((width, FH), BF),
            pltpu.VMEM((width, FH), BF),
            pltpu.VMEM((FH, width), BF),
            pltpu.VMEM((2, N_SP, 8, FH), BF),
            pltpu.VMEM((2, N_SP, 8, FH), BF),
            pltpu.VMEM((2, N_SP, 8, FH), BF),
            pltpu.VMEM((NZ, TILES, 8, width), BF),
            pltpu.VMEM((2, NZ, HALF, 8, QW), BF),
            pltpu.VMEM((2, NZ, TILES, 8, QW), BF),
            pltpu.VMEM((2, NZ, TILES, 8, QW), BF),
            pltpu.VMEM((NZ, TILES, 8, QW), BF),
            pltpu.VMEM((width, FH), BF),
            pltpu.VMEM((width, FH), BF),
            pltpu.VMEM((FH, width), BF),
            pltpu.SemaphoreType.DMA,
            pltpu.SemaphoreType.DMA((NZ,)),
            pltpu.SemaphoreType.DMA,
            pltpu.SemaphoreType.DMA((2, NZ)),
            pltpu.SemaphoreType.DMA((2, NZ)),
            pltpu.SemaphoreType.DMA,
            pltpu.SemaphoreType.DMA((3,)),
            pltpu.SemaphoreType.DMA,
            pltpu.SemaphoreType.DMA((2, NZ)),
            pltpu.SemaphoreType.DMA,
            pltpu.SemaphoreType.DMA((2, NZ)),
            pltpu.SemaphoreType.DMA,
            pltpu.SemaphoreType.DMA,
            pltpu.SemaphoreType.DMA,
        ],
        compiler_params=pltpu.CompilerParams(collective_id=0, has_side_effects=True),
        name="experts",
    )(send, w_gate, w_up, w_down)


def sent_to_all(shard, axis):
    peers = lax.axis_size(axis)
    return lax.all_to_all(
        jnp.broadcast_to(shard[None], (peers, *shard.shape)), axis, 0, 0, tiled=True
    )


def laid_out(parts, dim):
    parts = jnp.moveaxis(parts, 0, dim)
    shape = parts.shape
    return parts.reshape(*shape[:dim], shape[dim] * shape[dim + 1], *shape[dim + 2 :])


def collect(shard, axis, dim):
    parts = sent_to_all(shard, axis)
    return laid_out(parts, dim)


def split_up(shard, dim, peers):
    shape = shard.shape
    parts = shard.reshape(*shape[:dim], peers, shape[dim] // peers, *shape[dim + 1 :])
    return jnp.moveaxis(parts, dim, 0)


def summed_on_arrival(shard, axis, dim):
    parts = split_up(shard, dim, lax.axis_size(axis))
    arrived = lax.all_to_all(parts, axis, split_axis=0, concat_axis=0, tiled=True)
    return arrived.astype(jnp.float32).sum(axis=0)


def passed_along(block, axis, distance):
    devices = range(lax.axis_size(axis))
    route = [(i - distance, i) for i in devices if i - distance in devices]
    return lax.ppermute(block, axis, route)


def contract_rows(left_side, right_side):
    return lax.dot_general(
        left_side, right_side, (((0,), (0,)), ((), ())), preferred_element_type=jnp.float32
    )


def contract_cols(left_side, right_side):
    return lax.dot_general(
        left_side, right_side, (((1,), (1,)), ((), ())), preferred_element_type=jnp.float32
    )


def local(
    grad_out,
    resid,
    norm_gain,
    routes,
    route_weights,
    gate_weight,
    up_weight,
    down_weight,
    proj_weight,
    conv_sum,
    conv_gain,
    conv_taps,
    conv_value,
    conv_gate,
):
    tok_rows, model_width = resid.shape
    tp = lax.axis_index("tp")
    core = lax.axis_index("sp") % 2
    resid_f = resid.astype(F32)
    inv_rms = lax.rsqrt(jnp.mean(resid_f * resid_f, axis=-1, keepdims=True) + 1e-06)
    first_col = tp * QW
    resid_q = lax.dynamic_slice_in_dim(resid, first_col, QW, 1).astype(F32)
    gain_q = lax.dynamic_slice_in_dim(norm_gain, first_col, QW, 0)
    normed_q = (resid_q * inv_rms * gain_q).astype(BF)
    grad_q = lax.dynamic_slice_in_dim(grad_out, first_col, QW, 1)

    experts = lax.broadcasted_iota(jnp.int32, (N_SP, tok_rows), 0)
    hit0 = routes[:, 0][None, :] == experts
    hit1 = routes[:, 1][None, :] == experts
    named = hit0 | hit1
    weight_of = jnp.where(hit0, route_weights[:, 0][None, :], 0.0) + jnp.where(
        hit1, route_weights[:, 1][None, :], 0.0
    )
    earlier = (
        lax.broadcasted_iota(jnp.int32, (tok_rows, tok_rows), 0)
        < lax.broadcasted_iota(jnp.int32, (tok_rows, tok_rows), 1)
    ).astype(BF)
    rank = jnp.dot(named.astype(BF), earlier, preferred_element_type=F32).astype(jnp.int32)
    rank = jnp.where(named, rank, -1)
    lane8 = jnp.arange(8, dtype=jnp.int32)[None, :, None]
    slot_a = rank[:, None, :] == lane8
    slot_b = rank[:, None, :] == 8 + lane8 % 4
    slots = jnp.stack([slot_a, slot_b], axis=0)
    slot_weight = jnp.sum(jnp.where(slots, weight_of[None, :, None, :], 0.0), axis=-1, keepdims=True)
    chosen = slots.astype(BF).reshape(2 * N_SP * 8, tok_rows)
    picked_rows = jnp.dot(chosen, normed_q, preferred_element_type=F32).astype(BF)
    picked_cots = (
        slot_weight.reshape(2 * N_SP * 8, 1) * jnp.dot(chosen, grad_q, preferred_element_type=F32)
    ).astype(BF)
    n = N_SP * 8
    lower = (lax.broadcasted_iota(jnp.int32, (n, 1), 0) % 8) < 4
    mixed = jnp.where(lower, picked_rows[n:], picked_cots[n:])
    send = jnp.concatenate([picked_rows[:n], mixed, picked_cots[:n]], axis=0).reshape(3, N_SP, 8, QW)
    returned, gate_grad, up_grad, down_grad = run_experts(
        send, gate_weight[0], up_weight[0], down_weight[0]
    )
    returned = returned.reshape(2 * n, QW)
    owner = lane8 // 4 == core
    back_slots = jnp.stack([slot_a, slot_b & owner], axis=0).astype(BF).reshape(2 * n, tok_rows)
    normed_part_grad = contract_rows(back_slots, returned).astype(BF)
    normed_grad = collect(normed_part_grad, "tp", 1)
    feature_grad = normed_grad.astype(jnp.float32) * norm_gain
    cubed = inv_rms * inv_rms * inv_rms
    resid_grad = (
        grad_out.astype(jnp.float32)
        + inv_rms * feature_grad
        - resid_f * cubed * jnp.mean(resid_f * feature_grad, axis=-1, keepdims=True)
    ).astype(jnp.bfloat16)
    channels = conv_sum.shape[1]
    summed = conv_sum.astype(jnp.float32).reshape(tok_rows, channels // GROUP, GROUP)
    centre = summed - jnp.mean(summed, axis=-1, keepdims=True)
    inv_std = lax.rsqrt(jnp.mean(centre * centre, axis=-1, keepdims=True) + 1e-05)
    grouped = centre * inv_std
    chan_normed = grouped.reshape(tok_rows, channels)
    pre_act = chan_normed * conv_gain
    sigma_conv = jax.nn.sigmoid(pre_act)
    conv_out = (pre_act * sigma_conv).astype(jnp.bfloat16)
    proj_grad = summed_on_arrival(contract_rows(resid_grad, conv_out).astype(jnp.bfloat16), "sp", 0)
    out_grad = jnp.dot(resid_grad, proj_weight, preferred_element_type=jnp.float32)
    normal_grad = (
        out_grad * sigma_conv * (1.0 + pre_act * (1.0 - sigma_conv)) * conv_gain
    ).reshape(tok_rows, channels // GROUP, GROUP)
    sum_grad = inv_std * (
        normal_grad
        - jnp.mean(normal_grad, axis=-1, keepdims=True)
        - grouped * jnp.mean(normal_grad * grouped, axis=-1, keepdims=True)
    )
    sum_grad = sum_grad.reshape(tok_rows, channels)
    following = passed_along(sum_grad[: CONV_K - 1], "sp", -1)
    extended = jnp.concatenate([sum_grad, following], axis=0)
    gated_grad = lax.conv_general_dilated(
        extended[None],
        conv_taps[::-1][:, None, :],
        (1,),
        ((0, 0),),
        dimension_numbers=("NWC", "WIO", "NWC"),
        feature_group_count=channels,
        precision=lax.Precision.HIGHEST,
    )[0]
    sigma_gate = jax.nn.sigmoid(conv_gate.astype(jnp.float32))
    value_grad = (gated_grad * sigma_gate).astype(jnp.bfloat16)
    gate_input_grad = (
        gated_grad * conv_value.astype(jnp.float32) * sigma_gate * (1.0 - sigma_gate)
    ).astype(jnp.bfloat16)
    return (gate_grad[None], up_grad[None], down_grad[None], proj_grad, value_grad, gate_input_grad)


def solution(mesh):
    in_specs = (
        P("sp", None),
        P("sp", None),
        P(),
        P("sp", None),
        P("sp", None),
        P("sp", None, "tp"),
        P("sp", None, "tp"),
        P("sp", "tp", None),
        P(None, "tp"),
        P("sp", "tp"),
        P("tp"),
        P(None, "tp"),
        P("sp", "tp"),
        P("sp", "tp"),
    )
    out_specs = (
        P("sp", None, "tp"),
        P("sp", None, "tp"),
        P("sp", "tp", None),
        P("sp", "tp"),
        P("sp", "tp"),
        P("sp", "tp"),
    )
    return jax.shard_map(local, mesh=mesh, in_specs=in_specs, out_specs=out_specs, check_vma=False)
```

time: 214 us -> 186 us (0.87)
  matrix products: 39.9 us -> 6.18 us
  waiting for transfers between devices: 6.92 us -> 26.6 us
  Pallas kernels: 123 us -> 116 us
  other arithmetic: 9.48 us -> 5.4 us
  local copies, waits for them, and re-layouts: 16.4 us -> 12.9 us
    dot_general x5 -> x2, matrix products: 19.8 us -> 3.11 us  [contract_rows(): lax.dot_general(left_side, right_side, (((0,), (0,)), ((), ())), preferre...]
    dot_general x5 -> x0, matrix products: 14.9 us -> none  [the longest x3 7.11 us: contract_cols(): lax.dot_general(left_side, right_side, (((1,), (1,)), ((), ())), preferre...]
    all_to_all x1, waiting for transfers between devices: 0.5 us -> 13.2 us  [sent_to_all(): lax.all_to_all(jnp.broadcast_to(shard[None], (peers, *shard.shape)), axis...]
    pallas_call x2 -> x1, Pallas kernels: 123 us -> 116 us  [run_experts(): pl.pallas_call(experts_kernel, out_shape=(jax.ShapeDtypeStruct((2, N_SP,...]
    slice x8 -> x0, local copies, waits for them, and re-layouts: 5.38 us -> none  [the longest x1 4.11 us: expert_backward(): with_rows, with_cots = (tall[:2 * n], tall[n:])]
    all_to_all x1, waiting for transfers between devices: 6.41 us -> 10.3 us  [summed_on_arrival(): lax.all_to_all(parts, axis, split_axis=0, concat_axis=0, tiled=True)]
    ppermute x1, waiting for transfers between devices: 0.01 us -> 3.04 us  [passed_along(): return lax.ppermute(block, axis, route)]
    unnamed x44 -> x33, local copies, waits for them, and re-layouts: 5.79 us -> 8.17 us
  transfers between devices with their start and end apart: 3 -> 3, of which waited for: 2 -> 3; matrix products, arithmetic and copies ran while one was open for 10% -> 2% of each run, Pallas kernels for 0% -> 0%
where the time goes in v2:
time: 186 us; the launch traced here: 185 us
  Pallas kernels  116 us (62%)
  waiting for transfers between devices  26.6 us (14%)
  starting transfers between devices  17.2 us (9%)
  local copies, waits for them, and re-layouts  12.9 us (7%)
  matrix products  6.18 us (3%)
  other arithmetic  5.4 us (3%)
    pallas_call x1, Pallas kernels, run_experts(): pl.pallas_call(experts_kernel, out_shape=(jax.ShapeDtypeStruct((2, N_SP,...  116 us
    all_to_all x1, waiting for transfers between devices, sent_to_all(): lax.all_to_all(jnp.broadcast_to(shard[None], (peers, *shard.shape)), axis...  13.2 us
    all_to_all x1, starting transfers between devices, summed_on_arrival(): lax.all_to_all(parts, axis, split_axis=0, concat_axis=0, tiled=True)  10.4 us
    all_to_all x1, waiting for transfers between devices, summed_on_arrival(): lax.all_to_all(parts, axis, split_axis=0, concat_axis=0, tiled=True)  10.3 us
    unnamed x33, local copies, waits for them, and re-layouts  8.17 us
    all_to_all x1, starting transfers between devices, sent_to_all(): lax.all_to_all(jnp.broadcast_to(shard[None], (peers, *shard.shape)), axis...  4.39 us
  transfers between devices with their start and end apart: 3, of which 3 were waited for; matrix products, arithmetic and copies ran while one was open for 2% of the time, Pallas kernels for 0%

profile of v2, /device:TPU:1, one launch (start us, length us, event | category | flops | bytes accessed | tf_op | source)
XLA Modules:
  0.0 185.2 jit_solution(1801743808583873915)
XLA Ops:
  0.6 0.0 copy-start
  0.6 0.0 copy-start.5
  0.7 0.8 fusion.63
  1.5 0.8 fusion.64
  2.3 0.2 fusion.8
  2.5 0.3 broadcast_and_fusion
  2.7 0.3 select_reduce_fusion
  3.0 0.2 copy.38
  3.3 0.0 copy-done.5
  3.3 0.0 copy-start.10
  3.3 0.5 copy.39
  3.8 0.3 fusion
  4.1 0.1 copy.40
  4.2 0.1 mul.160
  4.3 0.0 copy-done.10
  4.3 0.1 dynamic_slice.10
  4.4 0.5 convolution_convert_fusion.1
  5.0 1.4 multiply_convert_fusion
  6.4 0.2 fusion.62
  6.6 1.2 pad_maximum_fusion
  7.8 115.9 %experts.1 = (bf16[2,64,8,512]{3,2,1,0:T(8,128)(2,1)}, bf16[2048,384]{1,0:T(8,128)(2,1)}, bf16[2048,384]{1,0:T(8,128)(2,1)}, bf16[384,2048]{1,0:T(8,128)(2,1)}) custom-call(bf16[3,64,8,512]{3,2,1,0:T(8,128)(2,1)} %bitcast.45, bf16[2048,384]{1,0:T(8,128)(2,1)} %bitcast.49, bf16[2048,384]{1,0:T(8,128)(2,1)} %bitcast.50, bf16[384,2048]{1,0:T(8,128)(2,1)} %bitcast.51), custom_call_target="tpu_custom_call" | custom-call | tf_op jit(solution)/shard_map/experts/pallas_call | solution.py:288
  123.8 1.8 fusion.5
  125.5 0.0 copy-start.6
  125.6 1.1 broadcast_in_dim.93
  126.6 0.0 copy-start.7
  126.6 4.4 %all-to-all-start = ((bf16[4,256,512]{2,1,0:T(8,128)(2,1)}), bf16[4,256,512]{2,1,0:T(8,128)(2,1)}, u32[]{:S(2)}, u32[]{:S(2)}) async-start(bf16[4,256,512]{2,1,0:T(8,128)(2,1)} %broadcast_in_dim.93), calls=%async_computation | async-start | bytes 2097152 | tf_op jit(solution)/shard_map/all_to_all | solution.py:336
  131.0 0.0 copy-done.6
  131.0 1.3 copy.41
  132.3 0.0 copy-done.7
  132.3 0.1 convert_reduce_fusion.1
  132.4 0.2 fusion.37
  132.6 13.2 %all-to-all-done = bf16[4,256,512]{2,1,0:T(8,128)(2,1)} async-done(((bf16[4,256,512]{2,1,0:T(8,128)(2,1)}), bf16[4,256,512]{2,1,0:T(8,128)(2,1)}, u32[]{:S(2)}, u32[]{:S(2)}) %all-to-all-start) | async-done | bytes 1048608 | tf_op jit(solution)/shard_map/all_to_all | solution.py:336
  145.9 1.5 copy.43
  147.3 0.0 copy-start.1
  147.4 0.4 fusion.4
  147.8 0.8 copy-done.1
  148.6 0.0 copy-start.12
  148.6 0.7 fusion.3
  149.3 0.0 copy-done.12
  149.3 1.4 convolution_convert_fusion
  150.6 0.0 copy-done
  150.6 0.0 copy-start.11
  150.6 0.6 fusion.61
  151.2 10.4 %all-to-all-start.1 = ((bf16[64,32,128]{2,1,0:T(8,128)(2,1)}), bf16[64,32,128]{2,1,0:T(8,128)(2,1)S(1)}, u32[]{:S(2)}, u32[]{:S(2)}) async-start(bf16[64,32,128]{2,1,0:T(8,128)(2,1)} %bitcast.16), calls=%async_computation.1 | async-start | bytes 1048576 | tf_op jit(solution)/shard_map/all_to_all | solution.py:360
  161.7 0.2 fusion.36
  161.9 2.4 %collective-permute-start = (f32[30,128]{1,0:T(8,128)S(1)}, f32[30,128]{1,0:T(8,128)S(1)}, u32[]{:S(2)}, u32[]{:S(2)}) collective-permute-start(f32[30,128]{1,0:T(8,128)S(1)} %slice.44), channel_id=1, source_target_pairs={{4,0},{8,4},{12,8},{16,12},{20,16},{24,20},{28,24},{32,28},{36,32}... | collective-permute-start | bytes 46088 | tf_op jit(solution)/shard_map/ppermute | solution.py:367
  164.3 0.0 copy-done.11
  164.3 3.0 %collective-permute-done = f32[30,128]{1,0:T(8,128)S(1)} collective-permute-done((f32[30,128]{1,0:T(8,128)S(1)}, f32[30,128]{1,0:T(8,128)S(1)}, u32[]{:S(2)}, u32[]{:S(2)}) %collective-permute-start) | collective-permute-done | bytes 15392 | tf_op jit(solution)/shard_map/ppermute | solution.py:367
  167.4 0.0 copy-done.13
  167.4 0.0 copy-start.8
  167.4 0.0 copy-start.9
  167.4 0.0 copy-start.4
  167.5 0.4 convolution_select_fusion
  167.9 0.4 copy-done.8
  168.3 0.0 copy-done.9
  168.3 0.7 multiply_convert_fusion.3
  169.0 10.3 %all-to-all-done.1 = bf16[64,32,128]{2,1,0:T(8,128)(2,1)S(1)} async-done(((bf16[64,32,128]{2,1,0:T(8,128)(2,1)}), bf16[64,32,128]{2,1,0:T(8,128)(2,1)S(1)}, u32[]{:S(2)}, u32[]{:S(2)}) %all-to-all-start.1) | async-done | bytes 524320 | tf_op jit(solution)/shard_map/all_to_all | solution.py:360
  179.4 0.7 convert_reduce_fusion
  180.1 0.0 copy-done.4
  180.1 1.1 copy.61
  181.2 0.8 copy-done.3
  182.0 1.1 copy.62
  183.2 0.8 copy-done.2
  184.0 1.1 copy.63
  (20 shorter events, 0.2 us)
Async XLA Ops:
  0.6 150.0 %copy-start = (bf16[2048,128]{1,0:T(8,128)(2,1)S(1)}, bf16[2048,128]{1,0:T(8,128)(2,1)}, u32[]{:S(2)}) copy-start(bf16[2048,128]{1,0:T(8,128)(2,1)} %param.22) | copy-start | bytes 1572868
  0.6 2.6 %copy-start.5 = (bf16[256,2048]{1,0:T(8,128)(2,1)S(1)}, bf16[256,2048]{1,0:T(8,128)(2,1)}, u32[]{:S(2)}) copy-start(bf16[256,2048]{1,0:T(8,128)(2,1)} %param.15) | copy-start | bytes 3145732
  3.3 1.1 copy-start.10
  125.5 5.5 %copy-start.6 = (bf16[256,2048]{1,0:T(8,128)(2,1)S(1)}, bf16[256,2048]{1,0:T(8,128)(2,1)}, u32[]{:S(2)}) copy-start(bf16[256,2048]{1,0:T(8,128)(2,1)} %param.14) | copy-start | bytes 3145732
  126.6 5.7 %copy-start.7 = (bf16[256,128]{1,0:T(8,128)(2,1)S(1)}, bf16[256,128]{1,0:T(8,128)(2,1)}, u32[]{:S(2)}) copy-start(bf16[256,128]{1,0:T(8,128)(2,1)} %param.23) | copy-start | bytes 196612
  126.6 19.3 %all-to-all-start = ((bf16[4,256,512]{2,1,0:T(8,128)(2,1)}), bf16[4,256,512]{2,1,0:T(8,128)(2,1)}, u32[]{:S(2)}, u32[]{:S(2)}) async-start(bf16[4,256,512]{2,1,0:T(8,128)(2,1)} %broadcast_in_dim.93), calls=%async_computation | async-start | bytes 2097152 | tf_op jit(solution)/shard_map/all_to_all | solution.py:336
  147.3 1.2 copy-start.1
  148.6 0.7 copy-start.12
  150.6 13.6 %copy-start.11 = (f32[31,128]{1,0:T(8,128)S(1)}, f32[31,128]{1,0:T(8,128)}, u32[]{:S(2)}) copy-start(f32[31,128]{1,0:T(8,128)} %param.25) | copy-start | bytes 47620
  151.2 16.2 %copy-start.13 = (pred[8,36]{0,1:T(8,128)(4,1)S(1)}, pred[8,36]{0,1:T(8,128)(4,1)}, u32[]{:S(2)}) copy-start(pred[8,36]{0,1:T(8,128)(4,1)} %constant.100) | copy-start | bytes 868
  151.2 28.1 %all-to-all-start.1 = ((bf16[64,32,128]{2,1,0:T(8,128)(2,1)}), bf16[64,32,128]{2,1,0:T(8,128)(2,1)S(1)}, u32[]{:S(2)}, u32[]{:S(2)}) async-start(bf16[64,32,128]{2,1,0:T(8,128)(2,1)} %bitcast.16), calls=%async_computation.1 | async-start | bytes 1048576 | tf_op jit(solution)/shard_map/all_to_all | solution.py:360
  161.9 5.4 %collective-permute-start = (f32[30,128]{1,0:T(8,128)S(1)}, f32[30,128]{1,0:T(8,128)S(1)}, u32[]{:S(2)}, u32[]{:S(2)}) collective-permute-start(f32[30,128]{1,0:T(8,128)S(1)} %slice.44), channel_id=1, source_target_pairs={{4,0},{8,4},{12,8},{16,12},{20,16},{24,20},{28,24},{32,28},{36,32}... | collective-permute-start | bytes 46088 | tf_op jit(solution)/shard_map/ppermute | solution.py:367
  167.4 0.8 copy-start.8
  167.4 0.9 copy-start.9
  167.4 12.6 %copy-start.4 = (bf16[2048,384]{1,0:T(8,128)(2,1)S(1)}, bf16[2048,384]{1,0:T(8,128)(2,1)}, u32[]{:S(2)}) copy-start(bf16[2048,384]{1,0:T(8,128)(2,1)} %get-tuple-element.10) | copy-start | bytes 4718596
  180.1 2.0 %copy-start.3 = (bf16[2048,384]{1,0:T(8,128)(2,1)S(1)}, bf16[2048,384]{1,0:T(8,128)(2,1)}, u32[]{:S(2)}) copy-start(bf16[2048,384]{1,0:T(8,128)(2,1)} %get-tuple-element.11) | copy-start | bytes 4718596
  182.0 2.0 %copy-start.2 = (bf16[384,2048]{1,0:T(8,128)(2,1)S(1)}, bf16[384,2048]{1,0:T(8,128)(2,1)}, u32[]{:S(2)}) copy-start(bf16[384,2048]{1,0:T(8,128)(2,1)} %get-tuple-element.12) | copy-start | bytes 4718596
